TPU v7x, 256 devices: a whole 4x4x8 slice. The times are simulated.
256 devices in a mesh: ep: 64 (over z, x, core), tp: 4 (over y).
Axes of the slice: x: 4, y: 4, z: 8, core: 2. Of those that a mesh axis runs over, the one named last changes fastest.
Arguments:
- queries: bfloat16 [8192, 2048], P('ep', 'tp'), may hold values from -60 to 60
- keys: bfloat16 [8192, 512], P('ep', 'tp'), may hold values from -60 to 60
- values: bfloat16 [8192, 512], P('ep', 'tp'), may hold values from -6 to 6
- cum_gates: float32 [8192, 16], P('ep', 'tp'), may hold values from -2051 to 0, as said below
- expert_in: bfloat16 [32768, 4096], P(('ep', 'tp')), may hold values from -6 to 6
- norm_gain: float32 [4096], replicated, may hold values from 0.1 to 1.9
- route_group: int32 [32768, 1], P(('ep', 'tp')), may hold values from 0 to 63; in each aligned block of 128 rows (0 to 127, 128 to 255, ...) at most 3 rows name the same one
- route_member: int32 [32768, 2], P(('ep', 'tp')), may hold values from 0 to 3, all different within a row
- route_weight: float32 [32768, 2], P(('ep', 'tp')), may hold values from 0.1 to 1
- w_gate: bfloat16 [256, 4096, 384], P(('ep', 'tp')), may hold values from -0.09375 to 0.09375
- w_up: bfloat16 [256, 4096, 384], P(('ep', 'tp')), may hold values from -0.09375 to 0.09375
- w_down: bfloat16 [256, 384, 4096], P(('ep', 'tp')), may hold values from -0.3125 to 0.3125
Outputs:
- attended: bfloat16 [8192, 2048], P('ep', 'tp')
- expert_out: bfloat16 [32768, 4096], P(('ep', 'tp'))
Inputs may be any that keep to these rules, and one draw needn't show every extreme that they name: `cum_gates`: each head's entries never rise along positions. `route_group`: at most 3 of the rows of one device name one group. `route_member`: the 2 entries of a row differ.
All inputs are finite; a program needn't handle non-finite values.
Results may differ from a plain program's by a relative error of at most 0.0075.
Values may be sent and summed in bfloat16 or wider, within the bound.
A program may use at most 128 MiB of HBM per device.

v0:
```python
import math

import jax
import jax.numpy as jnp
from jax import lax
from jax.sharding import PartitionSpec as P

HEAD_WIDTH = 128
GROUP = 4
TOP = 2


NEGATIVE = -1e30
EPSILON = 1e-06


def sent_together(arrays, axis, dim, along):
    ends, at = ([], 0)
    for a in arrays[:-1]:
        at += a.shape[along]
        ends.append(at)
    both = jnp.concatenate(arrays, axis=along)
    return tuple(jnp.split(lax.all_gather(both, axis, axis=dim, tiled=True), ends, axis=along))


def from_everyone(array, axis):
    length = lax.axis_size(axis)
    return lax.all_to_all(
        jnp.broadcast_to(array[None], (length, *array.shape)), axis, 0, 0, tiled=True
    )


def in_order(blocks, dim):
    blocks = jnp.moveaxis(blocks, 0, dim)
    shape = blocks.shape
    return blocks.reshape(*shape[:dim], shape[dim] * shape[dim + 1], *shape[dim + 2 :])


def gathered_copies(array, axis, dim):
    blocks = from_everyone(array, axis)
    return in_order(blocks, dim)


def group_fold(states, prepared_group, key_piece, value_piece, start_row, all_gates, key_heads):
    query_rows, query_pos, query_gates = prepared_group
    count_queries = query_rows.shape[0]
    head_count = all_gates.shape[1]
    heads_per_group = head_count // key_heads
    piece_rows = key_piece.shape[0]
    rows_per_block = math.gcd(piece_rows, 512)
    score_scale = HEAD_WIDTH ** (-0.5)

    def key_step(step_index, carried):
        running, totals, accumulated = carried
        offset = step_index * rows_per_block
        key_rows = lax.dynamic_slice_in_dim(key_piece, offset, rows_per_block, 0).reshape(
            rows_per_block, key_heads, HEAD_WIDTH
        )
        rows_of_value = lax.dynamic_slice_in_dim(value_piece, offset, rows_per_block, 0).reshape(
            rows_per_block, key_heads, HEAD_WIDTH
        )
        key_gates = lax.dynamic_slice_in_dim(all_gates, offset, rows_per_block, 0)
        key_pos = offset + jnp.arange(rows_per_block, dtype=jnp.int32)
        scores = jnp.einsum(
            "qgrd,kgd->grqk", query_rows, key_rows, preferred_element_type=jnp.float32
        )
        scores = scores.reshape(head_count, count_queries, rows_per_block) * score_scale
        scores = scores + query_gates.T[:, :, None] - key_gates.T[:, None, :]
        allowed = (key_pos[None, :] <= query_pos[:, None])[None]
        scores = jnp.where(allowed, scores, NEGATIVE)
        new_max = jnp.maximum(running, jnp.max(scores, axis=-1))
        weights = jnp.where(allowed, jnp.exp(scores - new_max[..., None]), 0.0)
        factor = jnp.exp(running - new_max)
        totals = totals * factor + jnp.sum(weights, axis=-1)
        inner_product = jnp.einsum(
            "tjub,btl->tjul",
            weights.astype(jnp.bfloat16).reshape(
                key_heads, heads_per_group, count_queries, rows_per_block
            ),
            rows_of_value,
            preferred_element_type=jnp.float32,
        )
        accumulated = accumulated * factor[..., None] + inner_product.reshape(
            head_count, count_queries, HEAD_WIDTH
        )
        return (new_max, totals, accumulated)

    def run_all(carried):
        return lax.fori_loop(0, piece_rows // rows_per_block, key_step, carried)

    def keep_state(carried):
        return carried

    return lax.cond(start_row <= query_pos[-1], run_all, keep_state, states)


def fold_attention(groups, keys, values, all_gates):
    key_heads = keys.shape[1] // HEAD_WIDTH
    head_count = all_gates.shape[1]
    prepared = []
    initial = []
    for query_block, query_pos in groups:
        count_queries = query_block.shape[0]
        prepared.append(
            (
                query_block.reshape(count_queries, key_heads, head_count // key_heads, HEAD_WIDTH),
                query_pos,
                all_gates[query_pos],
            )
        )
        initial.append(
            (
                jnp.full((head_count, count_queries), NEGATIVE, jnp.float32),
                jnp.zeros((head_count, count_queries), jnp.float32),
                jnp.zeros((head_count, count_queries, HEAD_WIDTH), jnp.float32),
            )
        )
    carried = tuple(initial)
    start_row = jnp.int32(0)
    key_piece, value_piece = sent_together((keys, values), "ep", 0, 1)
    finals = tuple(
        (
            group_fold(
                states, prepared_group, key_piece, value_piece, start_row, all_gates, key_heads
            )
            for states, prepared_group in zip(carried, prepared)
        )
    )
    outputs = []
    for running, totals, accumulated in finals:
        result = accumulated / totals[..., None]
        outputs.append(
            jnp.transpose(result, (1, 0, 2))
            .reshape(result.shape[1], head_count * HEAD_WIDTH)
            .astype(jnp.bfloat16)
        )
    return outputs


def attention_half(queries, keys, values, cum_gates):
    count_rows = queries.shape[0]
    head_count = cum_gates.shape[1]
    ep_index = lax.axis_index("ep")
    all_gates = gathered_copies(cum_gates, "ep", 0)
    query_heads = queries.reshape(count_rows, head_count, HEAD_WIDTH)
    positions = ep_index * count_rows + jnp.arange(count_rows, dtype=jnp.int32)
    outputs = fold_attention([(query_heads, positions)], keys, values, all_gates)
    attended = outputs[0]
    return attended


def expert_half(
    expert_in, norm_gain, route_group, route_member, route_weight, w_gate, w_up, w_down
):
    count_rows, model_width = expert_in.shape
    ep_size = lax.axis_size("ep")
    tp_size = lax.axis_size("tp")
    capacity = max(2, (3 * count_rows + 2 * ep_size - 1) // (2 * ep_size))
    floats = expert_in.astype(jnp.float32)
    normed = (
        floats * lax.rsqrt(jnp.mean(floats * floats, axis=-1, keepdims=True) + EPSILON) * norm_gain
    ).astype(jnp.bfloat16)
    members = jnp.arange(GROUP, dtype=jnp.int32)
    mix_weights = jnp.zeros((count_rows, GROUP), jnp.float32)
    for rank_index in range(TOP):
        mix_weights = mix_weights + route_weight[:, rank_index : rank_index + 1] * (
            route_member[:, rank_index : rank_index + 1] == members[None, :]
        ).astype(jnp.float32)
    mix_weights = mix_weights.astype(jnp.bfloat16)
    group_ids = route_group[:, 0]
    group_match = (group_ids[:, None] == jnp.arange(ep_size, dtype=jnp.int32)[None, :]).astype(
        jnp.int32
    )
    rank_within = jnp.sum((jnp.cumsum(group_match, axis=0) - group_match) * group_match, axis=1)
    slot_of_row = group_ids * capacity + rank_within
    row_of_slot = (
        jnp.full((ep_size * capacity,), count_rows, jnp.int32)
        .at[slot_of_row]
        .set(jnp.arange(count_rows, dtype=jnp.int32))
    )
    padded_rows = jnp.concatenate([normed, jnp.zeros((1, model_width), jnp.bfloat16)], axis=0)
    padded_weights = jnp.concatenate([mix_weights, jnp.zeros((1, GROUP), jnp.bfloat16)], axis=0)
    send_rows = padded_rows[row_of_slot].reshape(ep_size, capacity, model_width)
    send_weights = padded_weights[row_of_slot].reshape(ep_size, capacity, GROUP)
    gate_matrix = w_gate[0]
    up_matrix = w_up[0]
    down_matrix = w_down[0]
    arrived_rows = lax.all_to_all(send_rows, "ep", split_axis=0, concat_axis=0, tiled=True)
    arrived_weights = lax.all_to_all(send_weights, "ep", split_axis=0, concat_axis=0, tiled=True)
    sources = arrived_rows.shape[0]
    per_source = arrived_rows.shape[1]
    flat_rows = arrived_rows.reshape(sources * per_source, model_width)
    pieces = lax.all_gather(flat_rows, "tp", axis=0, tiled=True)
    gate_part = jnp.dot(pieces, gate_matrix, preferred_element_type=jnp.float32)
    up_part = jnp.dot(pieces, up_matrix, preferred_element_type=jnp.float32)
    hidden = (jax.nn.silu(gate_part) * up_part).astype(jnp.bfloat16)
    expert_outputs = jnp.dot(hidden, down_matrix, preferred_element_type=jnp.float32).astype(
        jnp.bfloat16
    )
    member_outputs = lax.all_to_all(
        expert_outputs.reshape(tp_size, sources * per_source, model_width),
        "tp",
        split_axis=0,
        concat_axis=0,
        tiled=True,
    )
    flat_weights = arrived_weights.reshape(sources * per_source, GROUP).astype(jnp.float32)
    combined = jnp.zeros((sources * per_source, model_width), jnp.float32)
    for member in range(GROUP):
        combined = combined + flat_weights[:, member : member + 1] * member_outputs[member]
    mixed = combined.astype(jnp.bfloat16).reshape(sources, per_source, model_width)
    returned = lax.all_to_all(mixed, "ep", split_axis=0, concat_axis=0, tiled=True)
    return returned.reshape(ep_size * capacity, model_width)[slot_of_row]


def per_device(
    queries,
    keys,
    values,
    cum_gates,
    expert_in,
    norm_gain,
    route_group,
    route_member,
    route_weight,
    w_gate,
    w_up,
    w_down,
):
    attended = attention_half(queries, keys, values, cum_gates)
    expert_out = expert_half(
        expert_in, norm_gain, route_group, route_member, route_weight, w_gate, w_up, w_down
    )
    return (attended, expert_out)


def solution(mesh):
    return jax.shard_map(
        per_device,
        mesh=mesh,
        in_specs=(
            P("ep", "tp"),
            P("ep", "tp"),
            P("ep", "tp"),
            P("ep", "tp"),
            P(("ep", "tp"), None),
            P(),
            P(("ep", "tp"), None),
            P(("ep", "tp"), None),
            P(("ep", "tp"), None),
            P(("ep", "tp"), None, None),
            P(("ep", "tp"), None, None),
            P(("ep", "tp"), None, None),
        ),
        out_specs=(P("ep", "tp"), P(("ep", "tp"), None)),
        check_vma=False,
    )
```

profile of v0, /device:TPU:1, one launch (start us, length us, event | category | flops | bytes accessed | tf_op | source)
XLA Modules:
  0.0 429.3 jit_solution(8995752138738827243)
XLA Ops:
  11.6 1.5 fusion.33
  13.2 1.6 fusion.35
  15.9 5.6 %gather_fusion.2 = bf16[192,4096]{1,0:T(8,128)(2,1)} fusion(bf16[129,4096]{1,0:T(8,128)(2,1)} %concatenate.11, s32[1024]{0:T(1024)S(1)} %pad_clamp_fusion.2), kind=kCustom, calls=%fused_computation.2 | custom fusion | bytes 3146496 | tf_op jit(solution)/shard_map/gather | solution.py:183
  21.4 4.1 reshape.160
  25.5 62.8 %all_to_all.25 = bf16[64,3,4096]{2,1,0:T(4,128)(2,1)} all-to-all(bf16[64,3,4096]{2,1,0:T(4,128)(2,1)} %reshape.160), channel_id=1, replica_groups=mesh['ep'=64,'tp'=4] {'ep'}, dimensions={0} | all-to-all | bytes 3145728 | tf_op jit(solution)/shard_map/all_to_all | solution.py:188
  88.3 4.3 reshape.161
  94.8 7.0 %all-to-all-start.1 = ((bf16[64,3,4]{1,2,0:T(4,128)(2,1)}), bf16[64,3,4]{1,2,0:T(4,128)(2,1)S(1)}, u32[]{:S(2)}, u32[]{:S(2)}) async-start(bf16[64,3,4]{1,2,0:T(4,128)(2,1)} %copy.46), calls=%async_computation.1 | async-start | bytes 131072 | tf_op jit(solution)/shard_map/all_to_all | solution.py:189
  101.7 56.8 %all-gather.5.cloned.1.call-done = bf16[768,4096]{1,0:T(8,128)(2,1)} async-done(((bf16[192,4096]{1,0:T(8,128)(2,1)}), bf16[768,4096]{1,0:T(8,128)(2,1)}) %all-gather.5.cloned.1.call-update) | async-done | bytes 6291472 | tf_op jit(solution)/shard_map/all_gather | solution.py:193
  158.6 6.6 %fusion.31 = f32[768,384]{1,0:T(8,128)S(1)} fusion(bf16[768,4096]{1,0:T(8,128)(2,1)} %all-gather.5.cloned.1.call-done, bf16[1,4096,384]{2,1,0:T(8,128)(2,1)} %param.25), kind=kOutput, calls=%fused_computation.51 | convolution fusion | flops 2415919104 | bytes 10616832 | tf_op jit(solution)/shard_map/dot_general | solution.py:194
  165.2 3.5 fusion.39
  168.7 5.3 %convolution_convert_fusion = bf16[768,4096]{1,0:T(8,128)(2,1)} fusion(bf16[768,384]{1,0:T(8,128)(2,1)S(1)} %fusion.39, bf16[1,384,4096]{2,1,0:T(8,128)(2,1)S(1)} %copy-done), kind=kOutput, calls=%fused_computation.46 | convolution fusion | flops 2419064832 | bytes 10027008 | tf_op jit(solution)/shard_map/dot_general | solution.py:197
  174.0 5.4 %all-to-all-start.3 = ((bf16[4,192,4096]{2,1,0:T(8,128)(2,1)}), bf16[4,192,4096]{2,1,0:T(8,128)(2,1)}, u32[]{:S(2)}, u32[]{:S(2)}) async-start(bf16[4,192,4096]{2,1,0:T(8,128)(2,1)} %bitcast.114), calls=%async_computation.3 | async-start | bytes 12582912 | tf_op jit(solution)/shard_map/all_to_all | solution.py:200
  181.1 68.9 %all-to-all-done.3 = bf16[4,192,4096]{2,1,0:T(8,128)(2,1)} async-done(((bf16[4,192,4096]{2,1,0:T(8,128)(2,1)}), bf16[4,192,4096]{2,1,0:T(8,128)(2,1)}, u32[]{:S(2)}, u32[]{:S(2)}) %all-to-all-start.3) | async-done | bytes 6291488 | tf_op jit(solution)/shard_map/all_to_all | solution.py:200
  250.6 11.7 %all-to-all-start = ((f32[64,128,4]{1,2,0:T(4,128)}), f32[64,128,4]{1,2,0:T(4,128)S(1)}, u32[]{:S(2)}, u32[]{:S(2)}) async-start(f32[64,128,4]{1,2,0:T(4,128)} %broadcast_in_dim.107), calls=%async_computation | async-start | bytes 262144 | tf_op jit(solution)/shard_map/all_to_all | solution.py:28
  262.3 7.3 %slice_convert_fusion.3 = (f32[1,192,4096]{2,1,0:T(8,128)}, f32[1,192,4096]{2,1,0:T(8,128)S(1)}, f32[1,192,4096]{2,1,0:T(8,128)}, f32[1,192,4096]{2,1,0:T(8,128)}) fusion(bf16[4,192,4096]{2,1,0:T(8,128)(2,1)} %all-to-all-done.3), kind=kLoop, calls=%fused_computation.61 | loop fusion | flops 3145728 | bytes 18874368 | tf_op jit(solution)/shard_map/convert_element_type | solution.py:210
  269.6 5.0 %reshape.166 = f32[64,3,4096]{2,1,0:T(4,128)} reshape(f32[1,192,4096]{2,1,0:T(8,128)} %get-tuple-element.375) | data formatting | bytes 6291456 | tf_op jit(solution)/shard_map/convert_element_type | solution.py:210
  274.6 5.0 %reshape.167 = f32[64,3,4096]{2,1,0:T(4,128)} reshape(f32[1,192,4096]{2,1,0:T(8,128)} %get-tuple-element.378) | data formatting | bytes 6291456 | tf_op jit(solution)/shard_map/convert_element_type | solution.py:210
  279.6 5.0 %reshape.168 = f32[64,3,4096]{2,1,0:T(4,128)} reshape(f32[1,192,4096]{2,1,0:T(8,128)} %get-tuple-element.377) | data formatting | bytes 6291456 | tf_op jit(solution)/shard_map/convert_element_type | solution.py:210
  284.6 3.0 reshape.169
  287.6 9.2 %add_convert_fusion = bf16[64,3,4096]{2,1,0:T(4,128)(2,1)} fusion(f32[64,3,4096]{2,1,0:T(4,128)} %reshape.169, f32[64,3,4096]{2,1,0:T(4,128)} %reshape.168, f32[64,3,4096]{2,1,0:T(4,128)} %reshape.167, f32[64,3,4096]{2,1,0:T(4,128)} %reshape.166, f32[64,3]{1,0:T(8,128)S(1)} %mul.184, f32[64,3]{1,0:T(8,128)S(1)} %mul.181, f32[64,3]{1,0:T(8,128)S(1)} %mul.178, ...), kind=kLoop, calls=%fused_computation.47 | loop fusion | flops 6291456 | bytes 14158848 | tf_op jit(solution)/shard_map/convert_element_type | solution.py:211
  296.9 10.6 %all-to-all-start.4 = ((bf16[64,3,4096]{2,1,0:T(4,128)(2,1)}), bf16[64,3,4096]{2,1,0:T(4,128)(2,1)}, u32[]{:S(2)}, u32[]{:S(2)}) async-start(bf16[64,3,4096]{2,1,0:T(4,128)(2,1)} %add_convert_fusion), calls=%async_computation.4 | async-start | bytes 4194304 | tf_op jit(solution)/shard_map/all_to_all | solution.py:212
  309.0 101.9 %conditional.1 = (f32[4,128]{1,0:T(4,128)}, f32[4,128,128]{2,1,0:T(8,128)}) conditional(s32[]{:T(128)} %bitcast.3, () %tuple.39, (bf16[8192,256]{1,0:T(8,128)(2,1)}, f32[64,128,4]{1,2,0:T(4,128)S(1)}, bf16[128,512]{1,0:T(8,128)(2,1)S(1)}, s32[]{:T(128)}, s32[128,1]{0,1:T(1,128)S(1)}, /*index=5*/s32[128,1]{0,1:T(1,128)S(1)}, s32[128]{0:T(128)S(1)}) %tuple.85), branch_computations={%region_0.0_spmd, %region_1.6_spmd} | conditional | flops 138940928 | bytes 13862235 | solution.py:94
  309.0 2.6 copy.42
  311.6 2.8 copy.41
  314.5 2.8 gather_fusion
  317.4 4.5 %fusion.47 = (bf16[8192,128]{1,0:T(8,128)(2,1)}, bf16[8192,128]{1,0:T(8,128)(2,1)}) fusion(bf16[8192,256]{1,0:T(8,128)(2,1)} %get-tuple-element.235), kind=kLoop, calls=%fused_computation.92 | loop fusion | bytes 8388608 | tf_op jit(solution)/shard_map/split | solution.py:23
  322.2 88.7 %while.23 = (s32[]{:T(128)}, f32[4,128]{1,0:T(4,128)S(1)}, f32[4,128]{1,0:T(4,128)}, f32[4,128,128]{2,1,0:T(8,128)}, s32[128]{0:T(128)S(1)}, /*index=5*/bf16[819...) while((s32[]{:T(128)}, f32[4,128]{1,0:T(4,128)S(1)}, ...), condition=%wide.region_5.5_spmd.clone, body=%wide.region_2.4_spmd.clone.sunk | while | flops 138939392 | bytes 4410063 | solution.py:89
  324.7 2.3 convolution_add_fusion.2
  330.2 2.4 convolution_add_fusion.2
  335.8 2.4 convolution_add_fusion.2
  341.4 2.4 convolution_add_fusion.2
  346.9 2.4 convolution_add_fusion.2
  352.5 2.4 convolution_add_fusion.2
  358.1 2.4 convolution_add_fusion.2
  363.7 2.4 convolution_add_fusion.2
  366.3 1.3 fusion.58
  369.3 2.4 convolution_add_fusion.2
  371.9 1.3 fusion.58
  374.9 2.4 convolution_add_fusion.2
  380.5 2.4 convolution_add_fusion.2
  386.1 2.4 convolution_add_fusion.2
  391.7 2.4 convolution_add_fusion.2
  397.3 2.4 convolution_add_fusion.2
  402.9 2.4 convolution_add_fusion.2
  408.5 2.4 convolution_add_fusion.2
  410.9 1.7 copy_bitcast_fusion
  412.6 4.4 %reshape.163 = bf16[192,4096]{1,0:T(8,128)(2,1)} reshape(bf16[64,3,4096]{2,1,0:T(4,128)(2,1)} %all-to-all-done.4) | data formatting | bytes 3145728 | tf_op jit(solution)/shard_map/reshape | solution.py:213
  417.0 4.8 %gather_fusion.3 = bf16[128,4096]{1,0:T(8,128)(2,1)} fusion(bf16[192,4096]{1,0:T(8,128)(2,1)} %reshape.163, s32[1024]{0:T(1024)S(1)} %pad_clamp_fusion.1), kind=kCustom, calls=%fused_computation.3 | custom fusion | bytes 2097664 | tf_op jit(solution)/shard_map/gather | solution.py:213
  (194 shorter events, 57.4 us)
Async XLA Ops:
  8.0 160.7 %copy-start = (bf16[1,384,4096]{2,1,0:T(8,128)(2,1)S(1)}, bf16[1,384,4096]{2,1,0:T(8,128)(2,1)}, u32[]{:S(2)}) copy-start(bf16[1,384,4096]{2,1,0:T(8,128)(2,1)} %param.27) | copy-start | bytes 9437188
  8.0 150.6 %all-gather.5.cloned.1.call-start = ((), (), s32[]{:S(2)}) async-start(), calls=%async_computation.6 | async-start | bytes 7864320 | tf_op jit(solution)/shard_map/all_gather | solution.py:193
  88.3 4.3 %copy-start.6 = (s32[128,2]{0,1:T(2,128)S(1)}, s32[128,2]{0,1:T(2,128)}, u32[]{:S(2)}) copy-start(s32[128,2]{0,1:T(2,128)} %param.23) | copy-start | bytes 3076
  88.3 4.3 %copy-start.7 = (f32[128,2]{0,1:T(2,128)S(1)}, f32[128,2]{0,1:T(2,128)}, u32[]{:S(2)}) copy-start(f32[128,2]{0,1:T(2,128)} %param.24) | copy-start | bytes 3076
  94.8 79.2 %all-to-all-start.1 = ((bf16[64,3,4]{1,2,0:T(4,128)(2,1)}), bf16[64,3,4]{1,2,0:T(4,128)(2,1)S(1)}, u32[]{:S(2)}, u32[]{:S(2)}) async-start(bf16[64,3,4]{1,2,0:T(4,128)(2,1)} %copy.46), calls=%async_computation.1 | async-start | bytes 131072 | tf_op jit(solution)/shard_map/all_to_all | solution.py:189
  158.6 6.6 %copy-start.8 = (bf16[768,4096]{1,0:T(8,128)(2,1)S(1)}, bf16[768,4096]{1,0:T(8,128)(2,1)}, u32[]{:S(2)}) copy-start(bf16[768,4096]{1,0:T(8,128)(2,1)} %all-gather.5.cloned.1.call-done) | copy-start | bytes 18874372
  158.6 6.6 %copy-start.9 = (bf16[1,4096,384]{2,1,0:T(8,128)(2,1)S(1)}, bf16[1,4096,384]{2,1,0:T(8,128)(2,1)}, u32[]{:S(2)}) copy-start(bf16[1,4096,384]{2,1,0:T(8,128)(2,1)} %param.26) | copy-start | bytes 9437188
  173.9 5.5 %copy-start.3 = (bf16[128,128]{1,0:T(8,128)(2,1)S(1)}, bf16[128,128]{1,0:T(8,128)(2,1)}, u32[]{:S(2)}) copy-start(bf16[128,128]{1,0:T(8,128)(2,1)} %param.18) | copy-start | bytes 98308
  174.0 5.5 %copy-start.4 = (bf16[128,128]{1,0:T(8,128)(2,1)S(1)}, bf16[128,128]{1,0:T(8,128)(2,1)}, u32[]{:S(2)}) copy-start(bf16[128,128]{1,0:T(8,128)(2,1)} %param.17) | copy-start | bytes 98308
  174.0 76.0 %copy-start.5 = (f32[128,4]{0,1:T(4,128)S(1)}, f32[128,4]{0,1:T(4,128)}, u32[]{:S(2)}) copy-start(f32[128,4]{0,1:T(4,128)} %param.19) | copy-start | bytes 6148
  174.0 76.0 %all-to-all-start.3 = ((bf16[4,192,4096]{2,1,0:T(8,128)(2,1)}), bf16[4,192,4096]{2,1,0:T(8,128)(2,1)}, u32[]{:S(2)}, u32[]{:S(2)}) async-start(bf16[4,192,4096]{2,1,0:T(8,128)(2,1)} %bitcast.114), calls=%async_computation.3 | async-start | bytes 12582912 | tf_op jit(solution)/shard_map/all_to_all | solution.py:200
  179.4 129.6 %all-gather.3.cloned.1.call-start = ((), (), s32[]{:S(2)}) async-start(), calls=%async_computation.5 | async-start | bytes 4259840 | tf_op jit(solution)/shard_map/all_gather | solution.py:23
  250.6 46.3 %all-to-all-start = ((f32[64,128,4]{1,2,0:T(4,128)}), f32[64,128,4]{1,2,0:T(4,128)S(1)}, u32[]{:S(2)}, u32[]{:S(2)}) async-start(f32[64,128,4]{1,2,0:T(4,128)} %broadcast_in_dim.107), calls=%async_computation | async-start | bytes 262144 | tf_op jit(solution)/shard_map/all_to_all | solution.py:28
  296.9 12.1 %copy-start.2 = (bf16[128,512]{1,0:T(8,128)(2,1)S(1)}, bf16[128,512]{1,0:T(8,128)(2,1)}, u32[]{:S(2)}) copy-start(bf16[128,512]{1,0:T(8,128)(2,1)} %param.16) | copy-start | bytes 393220
  296.9 115.7 %all-to-all-start.4 = ((bf16[64,3,4096]{2,1,0:T(4,128)(2,1)}), bf16[64,3,4096]{2,1,0:T(4,128)(2,1)}, u32[]{:S(2)}, u32[]{:S(2)}) async-start(bf16[64,3,4096]{2,1,0:T(4,128)(2,1)} %add_convert_fusion), calls=%async_computation.4 | async-start | bytes 4194304 | tf_op jit(solution)/shard_map/all_to_all | solution.py:212
  412.6 9.2 %copy-start.1 = (bf16[1,384,4096]{2,1,0:T(8,128)(2,1)S(1)}, bf16[1,384,4096]{2,1,0:T(8,128)(2,1)}, u32[]{:S(2)}) copy-start(bf16[1,384,4096]{2,1,0:T(8,128)(2,1)} %param.27) | copy-start | bytes 9437188
Sparse Core Ops, SparseCore 0:
  92.7 65.8 all-gather.4
Sparse Core Ops, SparseCore 1:
  183.2 81.4 all-gather.2
where the time goes:
time: 431 us; the launch traced here: 429 us
  waiting for transfers between devices  126 us (29%)
  matrix products  75 us (17%)
  blocking collectives  62.8 us (15%)
  local copies, waits for them, and re-layouts  60.7 us (14%)
  other arithmetic  53.2 us (12%)
  starting transfers between devices  34.8 us (8%)
  between operations  16.5 us (4%)
    all_to_all x1, waiting for transfers between devices, expert_half(): lax.all_to_all(expert_outputs.reshape(tp_size, sources * per_source, mode...  68.9 us
    all_to_all x1, blocking collectives, expert_half(): lax.all_to_all(send_rows, 'ep', split_axis=0, concat_axis=0, tiled=True)  62.8 us
    all_gather x1, waiting for transfers between devices, expert_half(): pieces = lax.all_gather(flat_rows, 'tp', axis=0, tiled=True)  56.8 us
    dot_general x16, matrix products, key_step(): jnp.einsum('tjub,btl->tjul', weights.astype(jnp.bfloat16).reshape(key_hea...  38.4 us
    dot_general x16, matrix products, key_step(): jnp.einsum('qgrd,kgd->grqk', query_rows, key_rows, preferred_element_type...  21.3 us
    add x16, other arithmetic, key_step(): totals = totals * factor + jnp.sum(weights, axis=-1)  20.1 us
    convert_element_type x4, local copies, waits for them, and re-layouts, expert_half(): flat_weights[:, member:member + 1] * member_outputs[member]  18 us
    all_to_all x1, starting transfers between devices, from_everyone(): lax.all_to_all(jnp.broadcast_to(array[None], (length, *array.shape)), axi...  11.7 us
  transfers between devices with their start and end apart: 6, of which 2 were waited for; matrix products, arithmetic and copies ran while one was open for 37% of the time, Pallas kernels for 0%

commit v1 on v0

v1 whole, which is shorter than its diff:
```python
import jax
import jax.numpy as jnp
from jax import lax
from jax.experimental import pallas as pl
from jax.experimental.pallas import tpu as pltpu
from jax.sharding import PartitionSpec as P

BF = jnp.bfloat16
F32 = jnp.float32
D = 4096
HALF = D // 2
FF = 384
HEAD = 128
HEADS = 4
ROWS = 128
CAP = 3
NZ, NX, NC = 8, 4, 2
NEP = 64
CHUNKS = 4
SLOTS = 48
MSG = CAP * 32
ORDER = (1, 7, 2, 5, 3, 4, 0, 6)
NEGATIVE = -1e30
EPSILON = 1e-06
SCALE = HEAD ** -0.5
Y_COPIES = 11


def dot(a, b):
    return jnp.dot(a, b, preferred_element_type=F32)


def iota(shape, dim):
    return lax.broadcasted_iota(jnp.int32, shape, dim)


def to_slots(read, store, perm_ref):
    columns = []
    for b in range(3):
        columns.append(
            jnp.concatenate([read(b, k) for k in range(32)], axis=0)
        )
    block = jnp.concatenate(columns, axis=1)
    for part in range(4):
        out = dot(perm_ref[part * 128 : (part + 1) * 128, :], block).astype(BF)
        for b in range(3):
            store(b * 512 + part * 128, out[:, b * 128 : (b + 1) * 128])


def from_slots(read, store, perm_ref):
    block = jnp.concatenate([read(b) for b in range(3)], axis=1)
    for part in range(4):
        out = dot(perm_ref[part * 128 : (part + 1) * 128, :], block).astype(BF)
        for i in range(8):
            for b in range(3):
                store(b, part * 8 + i, out[i * 16 : (i + 1) * 16, b * 128 : (b + 1) * 128])


def kernel(
    q_ref,
    keys_ref,
    values_ref,
    gates_ref,
    gates_t_ref,
    x_hbm,
    gain_ref,
    group_ref,
    member_ref,
    weight_ref,
    wg_hbm,
    wu_hbm,
    wd_hbm,
    att_ref,
    out_ref,
    x_ref,
    normed,
    gath,
    pick,
    place,
    perm_in,
    perm_out,
    send,
    recv,
    wsend,
    wrecv,
    xg,
    wgat,
    part,
    ra,
    rb,
    fl,
    fr,
    mixed,
    back,
    ret,
    total,
    hidden,
    wg,
    wu,
    wd,
    staged,
    kv,
    ga,
    load_sem,
    disp_send,
    disp_recv,
    w_send,
    w_recv,
    back_send,
    back_recv,
    kv_send,
    kv_recv,
    y_send,
    y_recv,
):
    me = lax.axis_index("ep")
    tp = lax.axis_index("tp")
    z = me // (NX * NC)
    xc = me % (NX * NC)
    x = xc // NC
    cc = xc % NC
    partner = me + 1 - 2 * cc
    right, left = (tp + 1) % 4, (tp + 3) % 4

    def ep_dev(e):
        return {"ep": e, "tp": tp}

    def tp_dev(t):
        return {"ep": me, "tp": t}

    barrier = pltpu.get_barrier_semaphore()

    @pl.loop(1, NEP)
    def _(i):
        pl.semaphore_signal(
            barrier, inc=1, device_id=ep_dev((me + i) % NEP), device_id_type=pl.DeviceIdType.MESH
        )

    for t in (right, left):
        pl.semaphore_signal(
            barrier, inc=1, device_id=tp_dev(t), device_id_type=pl.DeviceIdType.MESH
        )

    loads = [
        pltpu.make_async_copy(x_hbm, x_ref, load_sem.at[0]),
        pltpu.make_async_copy(keys_ref, staged.at[0], load_sem.at[1]),
        pltpu.make_async_copy(values_ref, staged.at[1], load_sem.at[2]),
        pltpu.make_async_copy(gates_t_ref, ga.at[z, xc], load_sem.at[3]),
        pltpu.make_async_copy(wg_hbm, wg, load_sem.at[4]),
        pltpu.make_async_copy(wu_hbm, wu, load_sem.at[5]),
        pltpu.make_async_copy(wd_hbm, wd, load_sem.at[6]),
    ]
    for c in loads:
        c.start()

    row, col = iota((512, 512), 0), iota((512, 512), 1)
    perm_in[...] = jnp.where((row & 31) * 16 + (row >> 5) == col, 1.0, 0.0).astype(BF)
    perm_out[...] = jnp.where((col & 31) * 16 + (col >> 5) == row, 1.0, 0.0).astype(BF)

    gid = group_ref[...]
    gz, gxc = gid >> 3, gid & 7
    gx, gc = gxc >> 1, gxc & 1
    dz, dx, dc = (gz - z) & 7, (gx - x) & 3, (gc + cc) & 1
    place_z = jnp.zeros_like(gid)
    for i, distance in enumerate(ORDER):
        place_z = place_z + jnp.where(dz == distance, i, 0)
    position = place_z * 8 + dx * 2 + dc
    lanes = iota((ROWS, ROWS), 1)
    match = jnp.where(position == lanes, 1.0, 0.0)
    below = jnp.where(iota((ROWS, ROWS), 0) > lanes, 1.0, 0.0).astype(BF)
    rank = jnp.sum(dot(below, match.astype(BF)) * match, axis=1, keepdims=True).astype(jnp.int32)
    slot = position * CAP + rank
    slots = jnp.where(slot == iota((ROWS, 256), 1), 1.0, 0.0)
    pick[...] = jnp.transpose(slots)[: CHUNKS * SLOTS].astype(BF)
    for c in range(CHUNKS):
        place[c] = jnp.where(slot - c * SLOTS == iota((ROWS, SLOTS), 1), 1.0, 0.0).astype(BF)
    lined = jnp.zeros((ROWS, ROWS), F32)
    for k in range(2):
        lane = rank * 4 + member_ref[:, k : k + 1]
        lined = lined + jnp.where(
            lanes == lane, weight_ref[:, k : k + 1].astype(BF).astype(F32), 0.0
        )
    wsend[...] = dot(jnp.transpose(match)[:NEP].astype(BF), lined.astype(BF)).reshape(NEP, 1, 128)

    loads[0].wait()

    @pl.loop(0, ROWS // 16)
    def _(i):
        at = pl.ds(pl.multiple_of(i * 16, 16), 16)
        floats = x_ref[at, :].astype(F32)
        mean = jnp.mean(floats * floats, axis=1, keepdims=True)
        normed[at, :] = (floats * lax.rsqrt(mean + EPSILON) * gain_ref[...]).astype(BF)

    @pl.loop(0, D // 512)
    def _(i):
        at = pl.ds(pl.multiple_of(i * 512, 512), 512)
        gath[:, at] = dot(pick[...], normed[:, at]).astype(BF)

    for c in loads[1:4]:
        c.wait()
    own = pltpu.make_async_copy(staged.at[cc], kv.at[cc, z, xc], load_sem.at[7])
    own.start()
    pl.semaphore_wait(barrier, NEP + 1)

    def remote(src, dst, ssem, rsem, dev):
        return pltpu.make_async_remote_copy(
            src_ref=src,
            dst_ref=dst,
            send_sem=ssem,
            recv_sem=rsem,
            device_id=dev,
            device_id_type=pl.DeviceIdType.MESH,
        )

    def wait_bytes(ref, sem):
        pltpu.make_async_copy(ref, ref, sem).wait()

    remote(
        staged.at[1 - cc], kv.at[1 - cc, z, xc], kv_send.at[0], kv_recv.at[0], ep_dev(partner)
    ).start()
    remote(ga.at[z, xc], ga.at[z, xc], kv_send.at[1], kv_recv.at[1], ep_dev(partner)).start()

    def message(p):
        return pl.ds(pl.multiple_of(p * MSG, MSG), MSG)

    def place_of(zi, j):
        dz = ORDER[zi]
        return (((z + dz) % NZ) * NX + (x + j // 2) % NX) * NC + (cc + j) % 2

    def place_from(zi, j):
        dz = ORDER[zi]
        return (((z + NZ - dz) % NZ) * NX + (x + NX - j // 2) % NX) * NC + (cc + j) % 2

    def for_partners(c, body):
        for zi in (2 * c, 2 * c + 1):

            @pl.loop(1 if ORDER[zi] == 0 else 0, 8)
            def _(j):
                body(zi, j, zi * 8 + j)

    own_place = ORDER.index(0) * 8
    own_chunk = own_place // 16
    own_rows = pl.ds(own_place * MSG, MSG)

    for c in range(CHUNKS):

        def read(b, k):
            return gath[c * SLOTS + b * 16 : c * SLOTS + (b + 1) * 16, k * 128 : (k + 1) * 128]

        def store(at, value):
            send[c * 1536 + at : c * 1536 + at + 128, :] = value

        to_slots(read, store, perm_in)

        def go(zi, j, p):
            remote(
                send.at[message(p)],
                recv.at[message(p)],
                disp_send,
                disp_recv.at[c],
                ep_dev(place_of(zi, j)),
            ).start()
            remote(
                wsend.at[p], wrecv.at[p], w_send, w_recv.at[c], ep_dev(place_of(zi, j))
            ).start()

        for_partners(c, go)
    pltpu.make_async_copy(send.at[own_rows], recv.at[own_rows], disp_recv.at[own_chunk]).start()
    pltpu.make_async_copy(
        wsend.at[own_place], wrecv.at[own_place], w_recv.at[own_chunk]
    ).start()

    own.wait()
    wait_bytes(staged.at[0], kv_recv.at[0])
    wait_bytes(ga.at[0, 0], kv_recv.at[1])
    pair = pl.ds(x * 2, 2)
    for dz in range(1, NZ):
        dev = ep_dev((me + dz * NX * NC) % NEP)
        remote(
            kv.at[cc, z, pair], kv.at[cc, z, pair], kv_send.at[2], kv_recv.at[2], dev
        ).start()
        remote(ga.at[z, pair], ga.at[z, pair], kv_send.at[3], kv_recv.at[3], dev).start()

    y_copies = {}

    def y_copy(c, i, src, dst, t):
        copy = remote(
            src, dst, y_send.at[c * Y_COPIES + i], y_recv.at[c * Y_COPIES + i], tp_dev(t)
        )
        copy.start()
        y_copies[c, i] = copy

    low, high = pl.ds(0, HALF), pl.ds(HALF, HALF)

    def gather_first(c):
        wait_bytes(recv.at[pl.ds(c * 1536, 1536)], disp_recv.at[c])
        wait_bytes(wrecv.at[pl.ds(c * 16, 16)], w_recv.at[c])

        def read(b):
            return recv[c * 1536 + b * 512 : c * 1536 + (b + 1) * 512, :]

        def store(b, k, value):
            xg[c, 0, b * 16 : (b + 1) * 16, k * 128 : (k + 1) * 128] = value

        from_slots(read, store, perm_out)
        wgat[c, 0] = wrecv[c * 16 : (c + 1) * 16]
        y_copy(c, 0, xg.at[c, 0], xg.at[c, 1], right)
        y_copy(c, 1, xg.at[c, 0], xg.at[c, 2], left)
        y_copy(c, 2, wgat.at[c, 0], wgat.at[c, 1], right)
        y_copy(c, 3, wgat.at[c, 0], wgat.at[c, 2], left)

    def gather_second(c):
        for i in range(4):
            y_copies[c, i].wait_recv()
        y_copy(c, 4, xg.at[c, 1, :, low], xg.at[c, 3, :, low], right)
        y_copy(c, 5, xg.at[c, 2, :, high], xg.at[c, 3, :, high], left)
        y_copy(c, 6, wgat.at[c, 1], wgat.at[c, 3], right)

    def experts(c):
        for i in range(4, 7):
            y_copies[c, i].wait_recv()
        rows = xg[c].reshape(4 * SLOTS, D)
        gate = dot(rows, wg[...])
        up = dot(rows, wu[...])
        hidden[...] = (gate / (1.0 + jnp.exp(-gate)) * up).astype(BF)
        i, j = iota((4 * SLOTS, 64), 0), iota((4 * SLOTS, 64), 1)
        spread = jnp.zeros((4 * SLOTS, 64), F32)
        for r in range(CAP):
            spread = spread + jnp.where(i == j * CAP + r, 1.0, 0.0)
        weights = dot(spread.astype(BF), wgat[c].reshape(64, 128).astype(BF))
        i, j = iota((4 * SLOTS, 128), 0), iota((4 * SLOTS, 128), 1)
        third = (i * 21846) >> 16
        mine = jnp.where(j == (i - third * CAP) * 4 + tp, weights, 0.0)
        column = jnp.sum(mine, axis=1, keepdims=True)

        @pl.loop(0, D // 512)
        def _(n):
            at = pl.ds(pl.multiple_of(n * 512, 512), 512)
            y = dot(hidden[...], wd[:, at]).astype(BF).astype(F32)
            part[c, :, :, at] = (y * column).astype(BF).reshape(4, SLOTS, 512)

        y_copy(c, 7, part.at[c, 3, :, low], ra.at[c], right)
        y_copy(c, 8, part.at[c, 3, :, high], rb.at[c], left)

    def reduce_second(c):
        y_copies[c, 7].wait_recv()
        y_copies[c, 8].wait_recv()

        @pl.loop(0, HALF // 512)
        def _(n):
            at = pl.ds(pl.multiple_of(n * 512, 512), 512)
            then = pl.ds(pl.multiple_of(n * 512 + HALF, 512), 512)
            part[c, 2, :, at] = (
                part[c, 2, :, at].astype(F32) + ra[c, :, at].astype(F32)
            ).astype(BF)
            part[c, 1, :, then] = (
                part[c, 1, :, then].astype(F32) + rb[c, :, at].astype(F32)
            ).astype(BF)

        y_copy(c, 9, part.at[c, 2], fl.at[c], right)
        y_copy(c, 10, part.at[c, 1], fr.at[c], left)

    def give_back(c):
        y_copies[c, 9].wait_recv()
        y_copies[c, 10].wait_recv()

        @pl.loop(0, D // 512)
        def _(n):
            at = pl.ds(pl.multiple_of(n * 512, 512), 512)
            mixed[:, at] = (
                part[c, 0, :, at].astype(F32)
                + fl[c, :, at].astype(F32)
                + fr[c, :, at].astype(F32)
            ).astype(BF)

        def read(b, k):
            return mixed[b * 16 : (b + 1) * 16, k * 128 : (k + 1) * 128]

        def store(at, value):
            back[c * 1536 + at : c * 1536 + at + 128, :] = value

        to_slots(read, store, perm_in)

        def go(zi, j, p):
            remote(
                back.at[message(p)],
                ret.at[message(p)],
                back_send,
                back_recv.at[c],
                ep_dev(place_from(zi, j)),
            ).start()

        for_partners(c, go)
        if c == own_chunk:
            pltpu.make_async_copy(
                back.at[own_rows], ret.at[own_rows], back_recv.at[own_chunk]
            ).start()

    def finish(c):
        wait_bytes(ret.at[pl.ds(c * 1536, 1536)], back_recv.at[c])

        def read(b):
            return ret[c * 1536 + b * 512 : c * 1536 + (b + 1) * 512, :]

        def store(b, k, value):
            mixed[b * 16 : (b + 1) * 16, k * 128 : (k + 1) * 128] = value

        from_slots(read, store, perm_out)

        @pl.loop(0, D // 512)
        def _(n):
            at = pl.ds(pl.multiple_of(n * 512, 512), 512)
            y = dot(place[c], mixed[:, at])
            if c > 0:
                y = y + total[:, at]
            if c < CHUNKS - 1:
                total[:, at] = y
            else:
                out_ref[:, at] = y.astype(BF)

    def attend(h):
        q = q_ref[:, h * HEAD : (h + 1) * HEAD]
        gate_q = gates_ref[:, h : h + 1]

        def step(kb, carried, masked):
            running, norm, acc = carried
            zi = kb // 2
            half = pl.ds((kb % 2) * 4, 4)
            k = kv[0, zi, half].reshape(512, HEAD)
            v = kv[1, zi, half].reshape(512, HEAD)
            gate_k = jnp.concatenate(
                [ga[zi, (kb % 2) * 4 + i, h : h + 1, :] for i in range(4)], axis=1
            )
            s = lax.dot_general(q, k, (((1,), (1,)), ((), ())), preferred_element_type=F32)
            s = s * SCALE + (gate_q - gate_k)
            if masked:
                allowed = iota((ROWS, 512), 1) + kb * 512 <= iota((ROWS, 512), 0) + me * ROWS
                s = jnp.where(allowed, s, NEGATIVE)
            top = jnp.maximum(running, jnp.max(s, axis=1, keepdims=True))
            w = jnp.exp(s - top)
            if masked:
                w = jnp.where(allowed, w, 0.0)
            factor = jnp.exp(running - top)
            norm = norm * factor + jnp.sum(w, axis=1, keepdims=True)
            acc = acc * factor + dot(w.astype(BF), v)
            return top, norm, acc

        carried = (
            jnp.full((ROWS, 1), NEGATIVE, F32),
            jnp.zeros((ROWS, 1), F32),
            jnp.zeros((ROWS, HEAD), F32),
        )
        last = me // 4
        carried = lax.fori_loop(0, last, lambda kb, s: step(kb, s, False), carried)
        _, norm, acc = step(last, carried, True)
        att_ref[:, h * HEAD : (h + 1) * HEAD] = (acc / norm).astype(BF)

    gather_first(0)

    wait_bytes(kv.at[0, pl.ds(0, 7), pl.ds(0, 2)], kv_recv.at[2])
    wait_bytes(ga.at[pl.ds(0, 7), pl.ds(0, 2)], kv_recv.at[3])
    for dx in range(1, NX):
        dev = ep_dev((z * NX + (x + dx) % NX) * NC + cc)
        remote(
            kv.at[cc, :, pair], kv.at[cc, :, pair], kv_send.at[4], kv_recv.at[4], dev
        ).start()
        remote(ga.at[:, pair], ga.at[:, pair], kv_send.at[5], kv_recv.at[5], dev).start()

    gather_first(1)
    gather_second(0)

    wait_bytes(kv.at[0, :, pl.ds(0, 6)], kv_recv.at[4])
    wait_bytes(ga.at[:, pl.ds(0, 6)], kv_recv.at[5])
    remote(kv.at[cc], kv.at[cc], kv_send.at[6], kv_recv.at[6], ep_dev(partner)).start()

    gather_first(2)
    for c in loads[4:7]:
        c.wait()
    experts(0)
    gather_second(1)
    wait_bytes(kv.at[0], kv_recv.at[6])
    attend(0)
    gather_first(3)
    reduce_second(0)
    experts(1)
    gather_second(2)
    attend(1)
    give_back(0)
    reduce_second(1)
    experts(2)
    gather_second(3)
    attend(2)
    reduce_second(2)
    give_back(1)
    experts(3)
    attend(3)
    give_back(2)
    reduce_second(3)
    finish(0)
    finish(1)
    give_back(3)
    finish(2)
    finish(3)

    for copy in y_copies.values():
        copy.wait_send()
    sent = pl.ds(0, (NEP - 1) * MSG)
    wait_bytes(send.at[sent], disp_send)
    wait_bytes(back.at[sent], back_send)
    wait_bytes(wsend.at[pl.ds(0, NEP - 1)], w_send)
    wait_bytes(staged.at[0], kv_send.at[0])
    wait_bytes(ga.at[0, 0], kv_send.at[1])
    wait_bytes(kv.at[0, pl.ds(0, 7), pl.ds(0, 2)], kv_send.at[2])
    wait_bytes(ga.at[pl.ds(0, 7), pl.ds(0, 2)], kv_send.at[3])
    wait_bytes(kv.at[0, :, pl.ds(0, 6)], kv_send.at[4])
    wait_bytes(ga.at[:, pl.ds(0, 6)], kv_send.at[5])
    wait_bytes(kv.at[0], kv_send.at[6])


def per_device(
    queries,
    keys,
    values,
    cum_gates,
    expert_in,
    norm_gain,
    route_group,
    route_member,
    route_weight,
    w_gate,
    w_up,
    w_down,
):
    vmem = pl.BlockSpec(memory_space=pltpu.VMEM)
    hbm = pl.BlockSpec(memory_space=pl.ANY)
    sem = pltpu.SemaphoreType.DMA
    scratch = [
        pltpu.VMEM((ROWS, D), BF),
        pltpu.VMEM((ROWS, D), BF),
        pltpu.VMEM((CHUNKS * SLOTS, D), BF),
        pltpu.VMEM((CHUNKS * SLOTS, ROWS), BF),
        pltpu.VMEM((CHUNKS, ROWS, SLOTS), BF),
        pltpu.VMEM((512, 512), BF),
        pltpu.VMEM((512, 512), BF),
        pltpu.VMEM((NEP * MSG, 128), BF),
        pltpu.VMEM((NEP * MSG, 128), BF),
        pltpu.VMEM((NEP, 1, 128), F32),
        pltpu.VMEM((NEP, 1, 128), F32),
        pltpu.VMEM((CHUNKS, 4, SLOTS, D), BF),
        pltpu.VMEM((CHUNKS, 4, 16, 1, 128), F32),
        pltpu.VMEM((CHUNKS, 4, SLOTS, D), BF),
        pltpu.VMEM((CHUNKS, SLOTS, HALF), BF),
        pltpu.VMEM((CHUNKS, SLOTS, HALF), BF),
        pltpu.VMEM((CHUNKS, SLOTS, D), BF),
        pltpu.VMEM((CHUNKS, SLOTS, D), BF),
        pltpu.VMEM((SLOTS, D), BF),
        pltpu.VMEM((NEP * MSG, 128), BF),
        pltpu.VMEM((NEP * MSG, 128), BF),
        pltpu.VMEM((ROWS, D), F32),
        pltpu.VMEM((4 * SLOTS, FF), BF),
        pltpu.VMEM((D, FF), BF),
        pltpu.VMEM((D, FF), BF),
        pltpu.VMEM((FF, D), BF),
        pltpu.VMEM((2, ROWS, HEAD), BF),
        pltpu.VMEM((2, NZ, NX * NC, ROWS, HEAD), BF),
        pltpu.VMEM((NZ, NX * NC, HEADS, ROWS), F32),
        sem((8,)),
        sem,
        sem((CHUNKS,)),
        sem,
        sem((CHUNKS,)),
        sem,
        sem((CHUNKS,)),
        sem((7,)),
        sem((7,)),
        sem((CHUNKS * Y_COPIES,)),
        sem((CHUNKS * Y_COPIES,)),
    ]
    return pl.pallas_call(
        kernel,
        name="step",
        out_shape=(
            jax.ShapeDtypeStruct((ROWS, HEADS * HEAD), BF),
            jax.ShapeDtypeStruct((ROWS, D), BF),
        ),
        in_specs=[vmem, hbm, hbm, vmem, hbm, hbm, vmem, vmem, vmem, vmem, hbm, hbm, hbm],
        out_specs=(vmem, vmem),
        scratch_shapes=scratch,
        compiler_params=pltpu.CompilerParams(
            collective_id=0, has_side_effects=True, vmem_limit_bytes=60 * 1024 * 1024
        ),
    )(
        queries,
        keys,
        values,
        cum_gates,
        cum_gates.T,
        expert_in,
        norm_gain.reshape(1, D),
        route_group,
        route_member,
        route_weight,
        w_gate[0],
        w_up[0],
        w_down[0],
    )


def solution(mesh):
    return jax.shard_map(
        per_device,
        mesh=mesh,
        in_specs=(
            P("ep", "tp"),
            P("ep", "tp"),
            P("ep", "tp"),
            P("ep", "tp"),
            P(("ep", "tp"), None),
            P(),
            P(("ep", "tp"), None),
            P(("ep", "tp"), None),
            P(("ep", "tp"), None),
            P(("ep", "tp"), None, None),
            P(("ep", "tp"), None, None),
            P(("ep", "tp"), None, None),
        ),
        out_specs=(P("ep", "tp"), P(("ep", "tp"), None)),
        check_vma=False,
    )
```

time: 431 us -> 200 us (0.46)
  Pallas kernels: 0 us -> 187 us
  waiting for transfers between devices: 126 us -> 0 us
  matrix products: 75 us -> 0 us
  blocking collectives: 62.8 us -> 0 us
  other arithmetic: 53.2 us -> 0 us
  local copies, waits for them, and re-layouts: 60.7 us -> 9.48 us
  starting transfers between devices: 34.8 us -> 0 us
  between operations: 16.5 us -> 0.64 us
    pallas_call x0 -> x1, Pallas kernels: none -> 187 us  [per_device(): pl.pallas_call(kernel, name='step', out_shape=(jax.ShapeDtypeStruct((ROWS...]
    dot_general x35 -> x0, matrix products: 75 us -> none  [the longest x16 38.4 us: key_step(): jnp.einsum('tjub,btl->tjul', weights.astype(jnp.bfloat16).reshape(key_hea...]
    all_to_all x4 -> x0, waiting for transfers between devices: 68.9 us -> none  [the longest x1 68.9 us: expert_half(): lax.all_to_all(expert_outputs.reshape(tp_size, sources * per_source, mode...]
    all_to_all x1 -> x0, blocking collectives: 62.8 us -> none  [expert_half(): lax.all_to_all(send_rows, 'ep', split_axis=0, concat_axis=0, tiled=True)]
    all_gather x2 -> x0, waiting for transfers between devices: 56.9 us -> none  [the longest x1 56.8 us: expert_half(): pieces = lax.all_gather(flat_rows, 'tp', axis=0, tiled=True)]
    all_to_all x4 -> x0, starting transfers between devices: 34.7 us -> none  [the longest x1 11.7 us: from_everyone(): lax.all_to_all(jnp.broadcast_to(array[None], (length, *array.shape)), axi...]
    convert_element_type x6 -> x0, other arithmetic: 20.9 us -> none  [the longest x1 9.24 us: expert_half(): combined.astype(jnp.bfloat16).reshape(sources, per_source, model_width)]
    add x33 -> x0, other arithmetic: 20.2 us -> none  [the longest x16 20.1 us: key_step(): totals = totals * factor + jnp.sum(weights, axis=-1)]
  transfers between devices with their start and end apart: 6 -> 0, of which waited for: 2 -> 0; matrix products, arithmetic and copies ran while one was open for 37% -> 0% of each run, Pallas kernels for 0% -> 0%
where the time goes in v1:
time: 200 us; the launch traced here: 197 us
  Pallas kernels  187 us (94%)
  local copies, waits for them, and re-layouts  9.48 us (5%)
    pallas_call x1, Pallas kernels, per_device(): pl.pallas_call(kernel, name='step', out_shape=(jax.ShapeDtypeStruct((ROWS...  187 us
    unnamed x6, local copies, waits for them, and re-layouts  9.48 us

profile of v1, /device:TPU:1, one launch (start us, length us, event | category | flops | bytes accessed | tf_op | source)
XLA Modules:
  0.0 197.1 jit_solution(15174961908252788548)
XLA Ops:
  0.6 1.4 copy.15.group_ref
  2.0 1.4 copy.16.member_ref
  3.4 1.4 copy.17.weight_ref
  4.8 1.4 copy.14.gates_ref
  6.3 187.0 %step.1 = (bf16[128,512]{1,0:T(8,128)(2,1)}, bf16[128,4096]{1,0:T(8,128)(2,1)}) custom-call(bf16[128,512]{1,0:T(8,128)(2,1)} %q_ref.1, bf16[128,128]{1,0:T(8,128)(2,1)} %keys_ref.1, bf16[128,128]{1,0:T(8,128)(2,1)} %values_ref.1, f32[128,4]{1,0:T(8,128)} %copy.14.gates_ref, f32[4,128]{1,0:T(4,128)} %bitcast.9, bf16[128,4096]{1,0:T(8,128)(2,1)} %x_hbm.1, ...), custom_call_target="tpu_custom_call" | custom-call | tf_op jit(solution)/shard_map/step/pallas_call | solution.py:579
  193.3 1.6 copy.20
  194.8 2.3 %copy.21 = bf16[128,4096]{1,0:T(8,128)(2,1)} copy(bf16[128,4096]{1,0:T(8,128)(2,1)} %get-tuple-element.5) | data formatting | bytes 2097152

commit v2 on v1

v2 whole, which is shorter than its diff:
```python
import jax
import jax.numpy as jnp
from jax import lax
from jax.experimental import pallas as pl
from jax.experimental.pallas import tpu as pltpu
from jax.sharding import PartitionSpec as P

BF = jnp.bfloat16
F32 = jnp.float32
D = 4096
HALF = D // 2
FF = 384
HEAD = 128
HEADS = 4
ROWS = 128
KEYS = 2048
CAP = 3
NZ, NX, NC = 8, 4, 2
NEP = 64
CHUNKS = 4
SLOTS = 48
LINES = 16
MSG = CAP * LINES
BLOCK = 16 * LINES
PART = 16 * MSG
ORDER = (1, 7, 3, 5, 2, 6, 0, 4)
NEGATIVE = -1e30
EPSILON = 1e-06
SCALE = HEAD ** -0.5
Y_COPIES = 15


def dot(a, b):
    return jnp.dot(a, b, preferred_element_type=F32)


def iota(shape, dim):
    return lax.broadcasted_iota(jnp.int32, shape, dim)


def to_slots(read, store, perm_ref):
    columns = []
    for b in range(3):
        columns.append(jnp.concatenate([read(b, k) for k in range(LINES)], axis=0))
    block = jnp.concatenate(columns, axis=1)
    for i in range(2):
        out = dot(perm_ref[i * 128 : (i + 1) * 128, :], block).astype(BF)
        for b in range(3):
            store(b * BLOCK + i * 128, out[:, b * 128 : (b + 1) * 128])


def from_slots(read, store, perm_ref):
    block = jnp.concatenate([read(b) for b in range(3)], axis=1)
    for i in range(2):
        out = dot(perm_ref[i * 128 : (i + 1) * 128, :], block).astype(BF)
        for k in range(8):
            for b in range(3):
                store(b, i * 8 + k, out[k * 16 : (k + 1) * 16, b * 128 : (b + 1) * 128])


def kernel(
    q_ref,
    keys_ref,
    values_ref,
    gates_hbm,
    x_hbm,
    gain_ref,
    group_ref,
    member_ref,
    weight_ref,
    wg_hbm,
    wu_hbm,
    wd_hbm,
    att_ref,
    out_ref,
    x_ref,
    normed,
    gath,
    pick,
    place,
    perm,
    send,
    recv,
    wsend,
    wrecv,
    xg,
    wgat,
    part,
    ra,
    rb,
    fl,
    fr,
    mixed,
    back,
    ret,
    total,
    hidden,
    wg,
    wu,
    wd,
    staged,
    kv,
    ga,
    load_sem,
    disp_send,
    disp_recv,
    w_send,
    w_recv,
    back_send,
    back_recv,
    kv_send,
    kv_recv,
    y_send,
    y_recv,
):
    me = lax.axis_index("ep")
    tp = lax.axis_index("tp")
    z = me // (NX * NC)
    xc = me % (NX * NC)
    x = xc // NC
    cc = xc % NC
    partner = me + 1 - 2 * cc
    right, left = (tp + 1) % 4, (tp + 3) % 4

    def ep_dev(e):
        return {"ep": e, "tp": tp}

    def tp_dev(t):
        return {"ep": me, "tp": t}

    barrier = pltpu.get_barrier_semaphore()

    @pl.loop(1, NEP)
    def _(i):
        pl.semaphore_signal(
            barrier, inc=1, device_id=ep_dev((me + i) % NEP), device_id_type=pl.DeviceIdType.MESH
        )

    for t in (right, left):
        pl.semaphore_signal(
            barrier, inc=1, device_id=tp_dev(t), device_id_type=pl.DeviceIdType.MESH
        )

    loads = [
        pltpu.make_async_copy(x_hbm, x_ref, load_sem.at[0]),
        pltpu.make_async_copy(keys_ref, staged.at[0], load_sem.at[1]),
        pltpu.make_async_copy(values_ref, staged.at[1], load_sem.at[2]),
        pltpu.make_async_copy(gates_hbm, ga.at[z, xc], load_sem.at[3]),
        pltpu.make_async_copy(wg_hbm, wg, load_sem.at[4]),
        pltpu.make_async_copy(wu_hbm, wu, load_sem.at[5]),
        pltpu.make_async_copy(wd_hbm, wd, load_sem.at[6]),
    ]
    for c in loads:
        c.start()

    row, col = iota((BLOCK, BLOCK), 0), iota((BLOCK, BLOCK), 1)
    perm[...] = jnp.where((row & 15) * 16 + (row >> 4) == col, 1.0, 0.0).astype(BF)

    facts = jnp.concatenate(
        [
            group_ref[...].astype(F32),
            member_ref[...].astype(F32),
            weight_ref[...],
            jnp.zeros((3, ROWS), F32),
        ],
        axis=0,
    )
    facts = jnp.transpose(facts)
    gid = facts[:, 0:1].astype(jnp.int32)
    gz, gxc = gid >> 3, gid & 7
    gx, gc = gxc >> 1, gxc & 1
    dz, dx, dc = (gz - z) & 7, (gx - x) & 3, (gc + cc) & 1
    place_z = jnp.zeros_like(gid)
    for i, distance in enumerate(ORDER):
        place_z = place_z + jnp.where(dz == distance, i, 0)
    position = place_z * 8 + dx * 2 + dc
    lanes = iota((ROWS, ROWS), 1)
    match = jnp.where(position == lanes, 1.0, 0.0)
    below = jnp.where(iota((ROWS, ROWS), 0) > lanes, 1.0, 0.0).astype(BF)
    rank = jnp.sum(dot(below, match.astype(BF)) * match, axis=1, keepdims=True).astype(jnp.int32)
    slot = position * CAP + rank
    slots = jnp.where(slot == iota((ROWS, 256), 1), 1.0, 0.0)
    pick[...] = jnp.transpose(slots)[: CHUNKS * SLOTS].astype(BF)
    for c in range(CHUNKS):
        place[c] = jnp.where(slot - c * SLOTS == iota((ROWS, SLOTS), 1), 1.0, 0.0).astype(BF)
    lined = jnp.zeros((ROWS, ROWS), F32)
    for k in range(2):
        lane = (position & 7) * 16 + rank * 4 + facts[:, 1 + k : 2 + k].astype(jnp.int32)
        lined = lined + jnp.where(
            lanes == lane, facts[:, 3 + k : 4 + k].astype(BF).astype(F32), 0.0
        )
    wsend[...] = dot(jnp.transpose(match)[:NEP].astype(BF), lined.astype(BF)).reshape(NEP, 1, 128)

    loads[0].wait()

    @pl.loop(0, ROWS // 16)
    def _(i):
        at = pl.ds(pl.multiple_of(i * 16, 16), 16)
        floats = x_ref[at, :].astype(F32)
        mean = jnp.mean(floats * floats, axis=1, keepdims=True)
        normed[at, :] = (floats * lax.rsqrt(mean + EPSILON) * gain_ref[...]).astype(BF)

    @pl.loop(0, D // 512)
    def _(i):
        at = pl.ds(pl.multiple_of(i * 512, 512), 512)
        gath[:, at] = dot(pick[...], normed[:, at]).astype(BF)

    for c in loads[1:4]:
        c.wait()
    gate_columns = jnp.transpose(
        jnp.concatenate([ga[z, xc], jnp.zeros((4, ROWS), F32)], axis=0)
    )
    own = pltpu.make_async_copy(staged.at[cc], kv.at[cc, z, xc], load_sem.at[7])
    own.start()
    pl.semaphore_wait(barrier, NEP + 1)

    def remote(src, dst, ssem, rsem, dev):
        return pltpu.make_async_remote_copy(
            src_ref=src,
            dst_ref=dst,
            send_sem=ssem,
            recv_sem=rsem,
            device_id=dev,
            device_id_type=pl.DeviceIdType.MESH,
        )

    def wait_bytes(ref, sem):
        pltpu.make_async_copy(ref, ref, sem).wait()

    remote(
        staged.at[1 - cc], kv.at[1 - cc, z, xc], kv_send.at[0], kv_recv.at[0], ep_dev(partner)
    ).start()
    remote(ga.at[z, xc], ga.at[z, xc], kv_send.at[1], kv_recv.at[1], ep_dev(partner)).start()

    pair = pl.ds(x * 2, 2)

    def kv_along_z():
        own.wait()
        wait_bytes(staged.at[0], kv_recv.at[0])
        wait_bytes(ga.at[0, 0], kv_recv.at[1])
        for dz in range(1, NZ):
            dev = ep_dev((me + dz * NX * NC) % NEP)
            remote(
                kv.at[cc, z, pair], kv.at[cc, z, pair], kv_send.at[2], kv_recv.at[2], dev
            ).start()
            remote(ga.at[z, pair], ga.at[z, pair], kv_send.at[3], kv_recv.at[3], dev).start()

    def kv_along_x():
        wait_bytes(kv.at[0, pl.ds(0, 7), pl.ds(0, 2)], kv_recv.at[2])
        wait_bytes(ga.at[pl.ds(0, 7), pl.ds(0, 2)], kv_recv.at[3])
        for dx in range(1, NX):
            dev = ep_dev((z * NX + (x + dx) % NX) * NC + cc)
            remote(
                kv.at[cc, :, pair], kv.at[cc, :, pair], kv_send.at[4], kv_recv.at[4], dev
            ).start()
            remote(ga.at[:, pair], ga.at[:, pair], kv_send.at[5], kv_recv.at[5], dev).start()

    def kv_across():
        wait_bytes(kv.at[0, :, pl.ds(0, 6)], kv_recv.at[4])
        wait_bytes(ga.at[:, pl.ds(0, 6)], kv_recv.at[5])
        remote(kv.at[cc], kv.at[cc], kv_send.at[6], kv_recv.at[6], ep_dev(partner)).start()

    def message(p):
        return pl.ds(pl.multiple_of(p * MSG, MSG), MSG)

    def place_of(zi, j):
        dz = ORDER[zi]
        return (((z + dz) % NZ) * NX + (x + j // 2) % NX) * NC + (cc + j) % 2

    def place_from(zi, j):
        dz = ORDER[zi]
        return (((z + NZ - dz) % NZ) * NX + (x + NX - j // 2) % NX) * NC + (cc + j) % 2

    def for_partners(c, body):
        for zi in (2 * c, 2 * c + 1):

            @pl.loop(1 if ORDER[zi] == 0 else 0, 8)
            def _(j):
                body(zi, j, zi * 8 + j)

    own_place = ORDER.index(0) * 8
    own_chunk = own_place // 16
    own_rows = pl.ds(own_place * MSG, MSG)

    for c in range(CHUNKS):
        for h in range(2):

            def read(b, k):
                k = h * LINES + k
                return gath[c * SLOTS + b * 16 : c * SLOTS + (b + 1) * 16, k * 128 : (k + 1) * 128]

            def store(at, value):
                send[h, c * PART + at : c * PART + at + 128, :] = value

            to_slots(read, store, perm)

            def go(zi, j, p):
                remote(
                    send.at[h, message(p)],
                    recv.at[h, message(p)],
                    disp_send,
                    disp_recv.at[2 * c + h],
                    ep_dev(place_of(zi, j)),
                ).start()
                if h == 0:
                    remote(
                        wsend.at[p], wrecv.at[p], w_send, w_recv.at[c], ep_dev(place_of(zi, j))
                    ).start()

            for_partners(c, go)
        if c == 2:
            kv_along_z()
    for h in range(2):
        pltpu.make_async_copy(
            send.at[h, own_rows], recv.at[h, own_rows], disp_recv.at[2 * own_chunk + h]
        ).start()
    pltpu.make_async_copy(
        wsend.at[own_place], wrecv.at[own_place], w_recv.at[own_chunk]
    ).start()

    y_copies = {}

    def y_copy(c, i, src, dst, t):
        copy = remote(
            src, dst, y_send.at[c * Y_COPIES + i], y_recv.at[c * Y_COPIES + i], tp_dev(t)
        )
        copy.start()
        y_copies[c, i] = copy

    def gather_first(c, h):
        wait_bytes(recv.at[h, pl.ds(c * PART, PART)], disp_recv.at[2 * c + h])

        def read(b):
            return recv[h, c * PART + b * BLOCK : c * PART + (b + 1) * BLOCK, :]

        def store(b, k, value):
            xg[c, h, 0, b * 16 : (b + 1) * 16, k * 128 : (k + 1) * 128] = value

        from_slots(read, store, perm)
        y_copy(c, 2 * h, xg.at[c, h, 0], xg.at[c, h, 1], right)
        y_copy(c, 2 * h + 1, xg.at[c, h, 0], xg.at[c, h, 2], left)
        if h == 1:
            wait_bytes(wrecv.at[pl.ds(c * 16, 16)], w_recv.at[c])
            wgat[c, 0] = jnp.sum(wrecv[c * 16 : (c + 1) * 16].reshape(2, 8, 128), axis=1)
            y_copy(c, 4, wgat.at[c, 0], wgat.at[c, 1], right)
            y_copy(c, 5, wgat.at[c, 0], wgat.at[c, 2], left)

    def gather_second(c, h):
        if h == 0:
            y_copies[c, 0].wait_recv()
            y_copy(c, 6, xg.at[c, 0, 1], xg.at[c, 0, 3], right)
        else:
            y_copies[c, 3].wait_recv()
            y_copy(c, 7, xg.at[c, 1, 2], xg.at[c, 1, 3], left)
            y_copies[c, 4].wait_recv()
            y_copy(c, 8, wgat.at[c, 1], wgat.at[c, 3], right)

    def experts(c):
        for i in (1, 2, 5, 6, 7, 8):
            y_copies[c, i].wait_recv()
        first = xg[c, 0].reshape(4 * SLOTS, HALF)
        second = xg[c, 1].reshape(4 * SLOTS, HALF)
        gate = dot(first, wg[:HALF, :]) + dot(second, wg[HALF:, :])
        up = dot(first, wu[:HALF, :]) + dot(second, wu[HALF:, :])
        hidden[...] = (gate / (1.0 + jnp.exp(-gate)) * up).astype(BF)
        i, j = iota((4 * SLOTS, 8), 0), iota((4 * SLOTS, 8), 1)
        spread = jnp.where((i * 2731) >> 16 == j, 1.0, 0.0).astype(BF)
        weights = dot(spread, wgat[c].reshape(8, 128).astype(BF))
        i, j = iota((4 * SLOTS, 128), 0), iota((4 * SLOTS, 128), 1)
        i = i - ((i * 2731) >> 16) * 24
        source = (i * 21846) >> 16
        lane = source * 16 + (i - source * CAP) * 4 + tp
        column = jnp.sum(jnp.where(j == lane, weights, 0.0), axis=1, keepdims=True)

        def down(h):
            @pl.loop(0, HALF // 512)
            def _(n):
                at = pl.ds(pl.multiple_of(n * 512, 512), 512)
                wide = pl.ds(pl.multiple_of(n * 512 + h * HALF, 512), 512)
                y = dot(hidden[...], wd[:, wide]).astype(BF).astype(F32)
                part[c, h, :, :, at] = (y * column).astype(BF).reshape(4, SLOTS, 512)

        down(0)
        y_copy(c, 9, part.at[c, 0, 3], ra.at[c], right)
        down(1)
        y_copy(c, 10, part.at[c, 1, 3], rb.at[c], left)
        y_copy(c, 11, part.at[c, 0, 1], fr.at[c, 0], left)

    def add_to(c, h, r, ref):
        @pl.loop(0, HALF // 512)
        def _(n):
            at = pl.ds(pl.multiple_of(n * 512, 512), 512)
            part[c, h, r, :, at] = (
                part[c, h, r, :, at].astype(F32) + ref[c, :, at].astype(F32)
            ).astype(BF)

    def reduce_second(c, h):
        y_copies[c, 9 + h].wait_recv()
        if h == 0:
            add_to(c, 0, 2, ra)
            y_copy(c, 12, part.at[c, 0, 2], fl.at[c, 0], right)
            y_copy(c, 13, part.at[c, 1, 2], fl.at[c, 1], right)
        else:
            add_to(c, 1, 1, rb)
            y_copy(c, 14, part.at[c, 1, 1], fr.at[c, 1], left)

    def give_back(c, h):
        y_copies[c, 12 + h].wait_recv()
        y_copies[c, 11 + 3 * h].wait_recv()

        @pl.loop(0, HALF // 512)
        def _(n):
            at = pl.ds(pl.multiple_of(n * 512, 512), 512)
            mixed[:, at] = (
                part[c, h, 0, :, at].astype(F32)
                + fl[c, h, :, at].astype(F32)
                + fr[c, h, :, at].astype(F32)
            ).astype(BF)

        def read(b, k):
            return mixed[b * 16 : (b + 1) * 16, k * 128 : (k + 1) * 128]

        def store(at, value):
            back[h, c * PART + at : c * PART + at + 128, :] = value

        to_slots(read, store, perm)

        def go(zi, j, p):
            remote(
                back.at[h, message(p)],
                ret.at[h, message(p)],
                back_send,
                back_recv.at[2 * c + h],
                ep_dev(place_from(zi, j)),
            ).start()

        for_partners(c, go)
        if c == own_chunk:
            pltpu.make_async_copy(
                back.at[h, own_rows], ret.at[h, own_rows], back_recv.at[2 * c + h]
            ).start()

    def finish(c, h):
        wait_bytes(ret.at[h, pl.ds(c * PART, PART)], back_recv.at[2 * c + h])

        def read(b):
            return ret[h, c * PART + b * BLOCK : c * PART + (b + 1) * BLOCK, :]

        def store(b, k, value):
            mixed[b * 16 : (b + 1) * 16, k * 128 : (k + 1) * 128] = value

        from_slots(read, store, perm)

        @pl.loop(0, HALF // 512)
        def _(n):
            at = pl.ds(pl.multiple_of(n * 512, 512), 512)
            wide = pl.ds(pl.multiple_of(n * 512 + h * HALF, 512), 512)
            y = dot(place[c], mixed[:, at])
            if c > 0:
                y = y + total[:, wide]
            if c < CHUNKS - 1:
                total[:, wide] = y
            else:
                out_ref[:, wide] = y.astype(BF)

    def attend(pair_of_heads):
        heads = (2 * pair_of_heads, 2 * pair_of_heads + 1)

        def step(kb, carried, masked):
            zs = pl.ds(kb * 2, 2)
            k = kv[0, zs].reshape(KEYS, HEAD)
            v = kv[1, zs].reshape(KEYS, HEAD)
            result = []
            for h, (running, norm, acc) in zip(heads, carried):
                q = q_ref[:, h * HEAD : (h + 1) * HEAD]
                gate_k = jnp.concatenate(
                    [ga[kb * 2 + i // 8, i % 8, h : h + 1, :] for i in range(16)], axis=1
                )
                s = lax.dot_general(q, k, (((1,), (1,)), ((), ())), preferred_element_type=F32)
                s = s * SCALE + (gate_columns[:, h : h + 1] - gate_k)
                if masked:
                    behind = me * ROWS - kb * KEYS
                    allowed = iota((ROWS, KEYS), 1) - iota((ROWS, KEYS), 0) <= behind
                    s = jnp.where(allowed, s, NEGATIVE)
                top = jnp.maximum(running, jnp.max(s, axis=1, keepdims=True))
                w = jnp.exp(s - top)
                if masked:
                    w = jnp.where(allowed, w, 0.0)
                factor = jnp.exp(running - top)
                norm = norm * factor + jnp.sum(w, axis=1, keepdims=True)
                acc = acc * factor + dot(w.astype(BF), v)
                result.append((top, norm, acc))
            return tuple(result)

        start = (
            jnp.full((ROWS, 1), NEGATIVE, F32),
            jnp.zeros((ROWS, 1), F32),
            jnp.zeros((ROWS, HEAD), F32),
        )
        last = me // 16
        carried = lax.fori_loop(0, last, lambda kb, c: step(kb, c, False), (start, start))
        for h, (_, norm, acc) in zip(heads, step(last, carried, True)):
            att_ref[:, h * HEAD : (h + 1) * HEAD] = (acc / norm).astype(BF)

    gather_first(0, 0)
    gather_first(0, 1)
    gather_second(0, 0)
    gather_second(0, 1)
    gather_first(1, 0)
    gather_first(1, 1)
    gather_first(2, 0)
    gather_first(2, 1)
    gather_second(1, 0)
    gather_second(1, 1)
    for c in loads[4:7]:
        c.wait()
    experts(0)
    gather_second(2, 0)
    gather_second(2, 1)
    experts(1)
    reduce_second(0, 0)
    gather_first(3, 0)
    kv_along_x()
    experts(2)
    reduce_second(1, 0)
    kv_across()
    gather_second(3, 0)
    give_back(0, 0)
    gather_first(3, 1)
    reduce_second(1, 1)
    gather_second(3, 1)
    reduce_second(2, 0)
    reduce_second(2, 1)
    give_back(1, 0)
    wait_bytes(kv.at[0], kv_recv.at[6])
    attend(1)
    reduce_second(0, 1)
    give_back(1, 1)
    experts(3)
    finish(0, 0)
    give_back(2, 0)
    give_back(0, 1)
    give_back(2, 1)
    reduce_second(3, 0)
    finish(1, 0)
    finish(2, 0)
    reduce_second(3, 1)
    give_back(3, 0)
    finish(0, 1)
    finish(1, 1)
    give_back(3, 1)
    finish(2, 1)
    attend(0)
    finish(3, 0)
    finish(3, 1)

    for copy in y_copies.values():
        copy.wait_send()
    sent = pl.ds(0, (NEP - 1) * MSG)
    wait_bytes(send.at[:, sent], disp_send)
    wait_bytes(back.at[:, sent], back_send)
    wait_bytes(wsend.at[pl.ds(0, NEP - 1)], w_send)
    wait_bytes(staged.at[0], kv_send.at[0])
    wait_bytes(ga.at[0, 0], kv_send.at[1])
    wait_bytes(kv.at[0, pl.ds(0, 7), pl.ds(0, 2)], kv_send.at[2])
    wait_bytes(ga.at[pl.ds(0, 7), pl.ds(0, 2)], kv_send.at[3])
    wait_bytes(kv.at[0, :, pl.ds(0, 6)], kv_send.at[4])
    wait_bytes(ga.at[:, pl.ds(0, 6)], kv_send.at[5])
    wait_bytes(kv.at[0], kv_send.at[6])


def per_device(
    queries,
    keys,
    values,
    cum_gates,
    expert_in,
    norm_gain,
    route_group,
    route_member,
    route_weight,
    w_gate,
    w_up,
    w_down,
):
    vmem = pl.BlockSpec(memory_space=pltpu.VMEM)
    hbm = pl.BlockSpec(memory_space=pl.ANY)
    sem = pltpu.SemaphoreType.DMA
    scratch = [
        pltpu.VMEM((ROWS, D), BF),
        pltpu.VMEM((ROWS, D), BF),
        pltpu.VMEM((CHUNKS * SLOTS, D), BF),
        pltpu.VMEM((CHUNKS * SLOTS, ROWS), BF),
        pltpu.VMEM((CHUNKS, ROWS, SLOTS), BF),
        pltpu.VMEM((BLOCK, BLOCK), BF),
        pltpu.VMEM((2, NEP * MSG, 128), BF),
        pltpu.VMEM((2, NEP * MSG, 128), BF),
        pltpu.VMEM((NEP, 1, 128), F32),
        pltpu.VMEM((NEP, 1, 128), F32),
        pltpu.VMEM((CHUNKS, 2, 4, SLOTS, HALF), BF),
        pltpu.VMEM((CHUNKS, 4, 2, 128), F32),
        pltpu.VMEM((CHUNKS, 2, 4, SLOTS, HALF), BF),
        pltpu.VMEM((CHUNKS, SLOTS, HALF), BF),
        pltpu.VMEM((CHUNKS, SLOTS, HALF), BF),
        pltpu.VMEM((CHUNKS, 2, SLOTS, HALF), BF),
        pltpu.VMEM((CHUNKS, 2, SLOTS, HALF), BF),
        pltpu.VMEM((SLOTS, HALF), BF),
        pltpu.VMEM((2, NEP * MSG, 128), BF),
        pltpu.VMEM((2, NEP * MSG, 128), BF),
        pltpu.VMEM((ROWS, D), F32),
        pltpu.VMEM((4 * SLOTS, FF), BF),
        pltpu.VMEM((D, FF), BF),
        pltpu.VMEM((D, FF), BF),
        pltpu.VMEM((FF, D), BF),
        pltpu.VMEM((2, ROWS, HEAD), BF),
        pltpu.VMEM((2, NZ, NX * NC, ROWS, HEAD), BF),
        pltpu.VMEM((NZ, NX * NC, HEADS, ROWS), F32),
        sem((8,)),
        sem,
        sem((2 * CHUNKS,)),
        sem,
        sem((CHUNKS,)),
        sem,
        sem((2 * CHUNKS,)),
        sem((7,)),
        sem((7,)),
        sem((CHUNKS * Y_COPIES,)),
        sem((CHUNKS * Y_COPIES,)),
    ]
    return pl.pallas_call(
        kernel,
        name="step",
        out_shape=(
            jax.ShapeDtypeStruct((ROWS, HEADS * HEAD), BF),
            jax.ShapeDtypeStruct((ROWS, D), BF),
        ),
        in_specs=[vmem, hbm, hbm, hbm, hbm, vmem, vmem, vmem, vmem, hbm, hbm, hbm],
        out_specs=(vmem, vmem),
        scratch_shapes=scratch,
        compiler_params=pltpu.CompilerParams(
            collective_id=0, has_side_effects=True, vmem_limit_bytes=60 * 1024 * 1024
        ),
    )(
        queries,
        keys,
        values,
        cum_gates.T,
        expert_in,
        norm_gain.reshape(1, D),
        route_group.T,
        route_member.T,
        route_weight.T,
        w_gate[0],
        w_up[0],
        w_down[0],
    )


def solution(mesh):
    return jax.shard_map(
        per_device,
        mesh=mesh,
        in_specs=(
            P("ep", "tp"),
            P("ep", "tp"),
            P("ep", "tp"),
            P("ep", "tp"),
            P(("ep", "tp"), None),
            P(),
            P(("ep", "tp"), None),
            P(("ep", "tp"), None),
            P(("ep", "tp"), None),
            P(("ep", "tp"), None, None),
            P(("ep", "tp"), None, None),
            P(("ep", "tp"), None, None),
        ),
        out_specs=(P("ep", "tp"), P(("ep", "tp"), None)),
        check_vma=False,
    )
```

time: 200 us -> 151 us (0.76); the launches traced: 197 us -> 151 us
  Pallas kernels: 187 us -> 147 us
  local copies, waits for them, and re-layouts: 9.48 us -> 3.85 us
    pallas_call x1, Pallas kernels: 187 us -> 147 us  [per_device(): pl.pallas_call(kernel, name='step', out_shape=(jax.ShapeDtypeStruct((ROWS...]
    unnamed x6 -> x2, local copies, waits for them, and re-layouts: 9.48 us -> 3.85 us
where the time goes in v2:
time: 151 us
  Pallas kernels  147 us (97%)
  local copies, waits for them, and re-layouts  3.85 us (3%)
    pallas_call x1, Pallas kernels, per_device(): pl.pallas_call(kernel, name='step', out_shape=(jax.ShapeDtypeStruct((ROWS...  147 us
    unnamed x2, local copies, waits for them, and re-layouts  3.85 us

profile of v2, /device:TPU:1, one launch (start us, length us, event | category | flops | bytes accessed | tf_op | source)
XLA Modules:
  0.0 151.2 jit_solution(12310969301947484088)
XLA Ops:
  0.6 146.7 %step.1 = (bf16[128,512]{1,0:T(8,128)(2,1)}, bf16[128,4096]{1,0:T(8,128)(2,1)}) custom-call(bf16[128,512]{1,0:T(8,128)(2,1)} %q_ref.1, bf16[128,128]{1,0:T(8,128)(2,1)} %keys_ref.1, bf16[128,128]{1,0:T(8,128)(2,1)} %values_ref.1, f32[4,128]{1,0:T(4,128)} %bitcast.12, bf16[128,4096]{1,0:T(8,128)(2,1)} %x_hbm.1, f32[1,4096]{1,0:T(1,128)} %bitcast.11, ...), custom_call_target="tpu_custom_call" | custom-call | tf_op jit(solution)/shard_map/step/pallas_call | solution.py:630
  147.3 1.6 %copy.16 = bf16[128,512]{1,0:T(8,128)(2,1)} copy(bf16[128,512]{1,0:T(8,128)(2,1)} %get-tuple-element.4) | data formatting | bytes 262144
  148.9 2.3 %copy.17 = bf16[128,4096]{1,0:T(8,128)(2,1)} copy(bf16[128,4096]{1,0:T(8,128)(2,1)} %get-tuple-element.5) | data formatting | bytes 2097152

commit v3 on v2

--- a/solution.py
+++ b/solution.py
@@ -193,23 +193,35 @@
 
     loads[0].wait()
 
-    @pl.loop(0, ROWS // 16)
+    @pl.loop(0, ROWS // 16, unroll=4)
     def _(i):
         at = pl.ds(pl.multiple_of(i * 16, 16), 16)
         floats = x_ref[at, :].astype(F32)
         mean = jnp.mean(floats * floats, axis=1, keepdims=True)
         normed[at, :] = (floats * lax.rsqrt(mean + EPSILON) * gain_ref[...]).astype(BF)
 
-    @pl.loop(0, D // 512)
-    def _(i):
-        at = pl.ds(pl.multiple_of(i * 512, 512), 512)
-        gath[:, at] = dot(pick[...], normed[:, at]).astype(BF)
-
+    def gather_rows(c):
+        rows = pl.ds(c * SLOTS, SLOTS)
+
+        @pl.loop(0, D // 512, unroll=2)
+        def _(i):
+            at = pl.ds(pl.multiple_of(i * 512, 512), 512)
+            gath[rows, at] = dot(pick[rows, :], normed[:, at]).astype(BF)
+
+        for h in range(2):
+
+            def read(b, k):
+                k = h * LINES + k
+                return gath[c * SLOTS + b * 16 : c * SLOTS + (b + 1) * 16, k * 128 : (k + 1) * 128]
+
+            def store(at, value):
+                send[h, c * PART + at : c * PART + at + 128, :] = value
+
+            to_slots(read, store, perm)
+
+    gather_rows(0)
     for c in loads[1:4]:
         c.wait()
-    gate_columns = jnp.transpose(
-        jnp.concatenate([ga[z, xc], jnp.zeros((4, ROWS), F32)], axis=0)
-    )
     own = pltpu.make_async_copy(staged.at[cc], kv.at[cc, z, xc], load_sem.at[7])
     own.start()
     pl.semaphore_wait(barrier, NEP + 1)
@@ -226,11 +238,6 @@
 
     def wait_bytes(ref, sem):
         pltpu.make_async_copy(ref, ref, sem).wait()
-
-    remote(
-        staged.at[1 - cc], kv.at[1 - cc, z, xc], kv_send.at[0], kv_recv.at[0], ep_dev(partner)
-    ).start()
-    remote(ga.at[z, xc], ga.at[z, xc], kv_send.at[1], kv_recv.at[1], ep_dev(partner)).start()
 
     pair = pl.ds(x * 2, 2)
 
@@ -283,16 +290,9 @@
     own_rows = pl.ds(own_place * MSG, MSG)
 
     for c in range(CHUNKS):
+        if c > 0:
+            gather_rows(c)
         for h in range(2):
-
-            def read(b, k):
-                k = h * LINES + k
-                return gath[c * SLOTS + b * 16 : c * SLOTS + (b + 1) * 16, k * 128 : (k + 1) * 128]
-
-            def store(at, value):
-                send[h, c * PART + at : c * PART + at + 128, :] = value
-
-            to_slots(read, store, perm)
 
             def go(zi, j, p):
                 remote(
@@ -308,6 +308,11 @@
                     ).start()
 
             for_partners(c, go)
+        if c == 0:
+            remote(
+                staged.at[1 - cc], kv.at[1 - cc, z, xc], kv_send.at[0], kv_recv.at[0], ep_dev(partner)
+            ).start()
+            remote(ga.at[z, xc], ga.at[z, xc], kv_send.at[1], kv_recv.at[1], ep_dev(partner)).start()
         if c == 2:
             kv_along_z()
     for h in range(2):
@@ -465,6 +470,9 @@
 
     def attend(pair_of_heads):
         heads = (2 * pair_of_heads, 2 * pair_of_heads + 1)
+        gate_columns = jnp.transpose(
+            jnp.concatenate([ga[z, xc], jnp.zeros((4, ROWS), F32)], axis=0)
+        )
 
         def step(kb, carried, masked):
             zs = pl.ds(kb * 2, 2)
@@ -510,44 +518,44 @@
     gather_first(1, 1)
     gather_first(2, 0)
     gather_first(2, 1)
-    gather_second(1, 0)
-    gather_second(1, 1)
     for c in loads[4:7]:
         c.wait()
     experts(0)
+    gather_second(1, 0)
+    gather_second(1, 1)
+    gather_second(2, 1)
+    reduce_second(0, 0)
+    kv_along_x()
+    give_back(0, 0)
+    gather_first(3, 0)
+    gather_first(3, 1)
+    experts(1)
     gather_second(2, 0)
-    gather_second(2, 1)
-    experts(1)
-    reduce_second(0, 0)
-    gather_first(3, 0)
-    kv_along_x()
-    experts(2)
+    reduce_second(0, 1)
+    finish(0, 0)
     reduce_second(1, 0)
-    kv_across()
-    gather_second(3, 0)
-    give_back(0, 0)
-    gather_first(3, 1)
     reduce_second(1, 1)
     gather_second(3, 1)
+    experts(2)
+    give_back(1, 0)
+    gather_second(3, 0)
+    give_back(0, 1)
+    kv_across()
+    give_back(1, 1)
     reduce_second(2, 0)
-    reduce_second(2, 1)
-    give_back(1, 0)
     wait_bytes(kv.at[0], kv_recv.at[6])
     attend(1)
-    reduce_second(0, 1)
-    give_back(1, 1)
+    finish(1, 0)
+    reduce_second(2, 1)
     experts(3)
-    finish(0, 0)
     give_back(2, 0)
-    give_back(0, 1)
     give_back(2, 1)
+    finish(0, 1)
     reduce_second(3, 0)
-    finish(1, 0)
-    finish(2, 0)
     reduce_second(3, 1)
     give_back(3, 0)
-    finish(0, 1)
     finish(1, 1)
+    finish(2, 0)
     give_back(3, 1)
     finish(2, 1)
     attend(0)
@@ -631,8 +639,8 @@
         kernel,
         name="step",
         out_shape=(
-            jax.ShapeDtypeStruct((ROWS, HEADS * HEAD), BF),
-            jax.ShapeDtypeStruct((ROWS, D), BF),
+            pltpu.VMEM((ROWS, HEADS * HEAD), BF),
+            pltpu.VMEM((ROWS, D), BF),
         ),
         in_specs=[vmem, hbm, hbm, hbm, hbm, vmem, vmem, vmem, vmem, hbm, hbm, hbm],
         out_specs=(vmem, vmem),

time: 151 us -> 141 us (0.934)
  Pallas kernels: 147 us -> 139 us
  local copies, waits for them, and re-layouts: 3.85 us -> 1.63 us
    pallas_call x1, Pallas kernels: 147 us -> 139 us  [per_device(): pl.pallas_call(kernel, name='step', out_shape=(pltpu.VMEM((ROWS, HEADS *...]
    unnamed x2, local copies, waits for them, and re-layouts: 3.85 us -> 1.63 us
where the time goes in v3:
time: 141 us
  Pallas kernels  139 us (99%)
  local copies, waits for them, and re-layouts  1.63 us (1%)
    pallas_call x1, Pallas kernels, per_device(): pl.pallas_call(kernel, name='step', out_shape=(pltpu.VMEM((ROWS, HEADS *...  139 us

profile of v3, /device:TPU:1, one launch (start us, length us, event | category | flops | bytes accessed | tf_op | source)
XLA Modules:
  0.0 141.0 jit_solution(5233045538607761068)
XLA Ops:
  0.6 138.7 %step.1 = (bf16[128,512]{1,0:T(8,128)(2,1)S(1)}, bf16[128,4096]{1,0:T(8,128)(2,1)S(1)}) custom-call(bf16[128,512]{1,0:T(8,128)(2,1)} %q_ref.1, bf16[128,128]{1,0:T(8,128)(2,1)} %keys_ref.1, bf16[128,128]{1,0:T(8,128)(2,1)} %values_ref.1, f32[4,128]{1,0:T(4,128)} %bitcast.12, bf16[128,4096]{1,0:T(8,128)(2,1)} %x_hbm.1, f32[1,4096]{1,0:T(1,128)} %bitcast.11, ...), custom_call_target="tpu_custom_call" | custom-call | tf_op jit(solution)/shard_map/step/pallas_call | solution.py:638
  139.3 0.7 copy.16
  140.0 1.0 copy.17

commit v4 on v3

--- a/solution.py
+++ b/solution.py
@@ -23,7 +23,7 @@
 MSG = CAP * LINES
 BLOCK = 16 * LINES
 PART = 16 * MSG
-ORDER = (1, 7, 3, 5, 2, 6, 0, 4)
+ORDER = (0, 6, 2, 4, 3, 5, 1, 7)
 NEGATIVE = -1e30
 EPSILON = 1e-06
 SCALE = HEAD ** -0.5
@@ -59,20 +59,25 @@
 
 
 def kernel(
-    q_ref,
+    q_hbm,
     keys_ref,
     values_ref,
     gates_hbm,
     x_hbm,
-    gain_ref,
-    group_ref,
-    member_ref,
-    weight_ref,
+    gain_hbm,
+    group_hbm,
+    member_hbm,
+    weight_hbm,
     wg_hbm,
     wu_hbm,
     wd_hbm,
     att_ref,
     out_ref,
+    q_ref,
+    gain_ref,
+    group_ref,
+    member_ref,
+    weight_ref,
     x_ref,
     normed,
     gath,
@@ -128,6 +133,31 @@
     def tp_dev(t):
         return {"ep": me, "tp": t}
 
+    quarters = [pl.ds(i * 32, 32) for i in range(4)]
+    x_loads = [
+        pltpu.make_async_copy(x_hbm.at[at], x_ref.at[at], load_sem.at[i])
+        for i, at in enumerate(quarters)
+    ]
+    facts_loads = [
+        pltpu.make_async_copy(group_hbm, group_ref, load_sem.at[4]),
+        pltpu.make_async_copy(member_hbm, member_ref, load_sem.at[5]),
+        pltpu.make_async_copy(weight_hbm, weight_ref, load_sem.at[6]),
+        pltpu.make_async_copy(gain_hbm, gain_ref, load_sem.at[7]),
+    ]
+    kv_loads = [
+        pltpu.make_async_copy(keys_ref, staged.at[0], load_sem.at[8]),
+        pltpu.make_async_copy(values_ref, staged.at[1], load_sem.at[9]),
+        pltpu.make_async_copy(gates_hbm, ga.at[z, xc], load_sem.at[10]),
+    ]
+    late_loads = [
+        pltpu.make_async_copy(wg_hbm, wg, load_sem.at[11]),
+        pltpu.make_async_copy(wu_hbm, wu, load_sem.at[12]),
+        pltpu.make_async_copy(wd_hbm, wd, load_sem.at[13]),
+        pltpu.make_async_copy(q_hbm, q_ref, load_sem.at[14]),
+    ]
+    for copy in facts_loads + x_loads + kv_loads:
+        copy.start()
+
     barrier = pltpu.get_barrier_semaphore()
 
     @pl.loop(1, NEP)
@@ -141,21 +171,11 @@
             barrier, inc=1, device_id=tp_dev(t), device_id_type=pl.DeviceIdType.MESH
         )
 
-    loads = [
-        pltpu.make_async_copy(x_hbm, x_ref, load_sem.at[0]),
-        pltpu.make_async_copy(keys_ref, staged.at[0], load_sem.at[1]),
-        pltpu.make_async_copy(values_ref, staged.at[1], load_sem.at[2]),
-        pltpu.make_async_copy(gates_hbm, ga.at[z, xc], load_sem.at[3]),
-        pltpu.make_async_copy(wg_hbm, wg, load_sem.at[4]),
-        pltpu.make_async_copy(wu_hbm, wu, load_sem.at[5]),
-        pltpu.make_async_copy(wd_hbm, wd, load_sem.at[6]),
-    ]
-    for c in loads:
-        c.start()
-
     row, col = iota((BLOCK, BLOCK), 0), iota((BLOCK, BLOCK), 1)
     perm[...] = jnp.where((row & 15) * 16 + (row >> 4) == col, 1.0, 0.0).astype(BF)
 
+    for copy in facts_loads:
+        copy.wait()
     facts = jnp.concatenate(
         [
             group_ref[...].astype(F32),
@@ -181,8 +201,6 @@
     slot = position * CAP + rank
     slots = jnp.where(slot == iota((ROWS, 256), 1), 1.0, 0.0)
     pick[...] = jnp.transpose(slots)[: CHUNKS * SLOTS].astype(BF)
-    for c in range(CHUNKS):
-        place[c] = jnp.where(slot - c * SLOTS == iota((ROWS, SLOTS), 1), 1.0, 0.0).astype(BF)
     lined = jnp.zeros((ROWS, ROWS), F32)
     for k in range(2):
         lane = (position & 7) * 16 + rank * 4 + facts[:, 1 + k : 2 + k].astype(jnp.int32)
@@ -191,7 +209,10 @@
         )
     wsend[...] = dot(jnp.transpose(match)[:NEP].astype(BF), lined.astype(BF)).reshape(NEP, 1, 128)
 
-    loads[0].wait()
+    for copy in x_loads:
+        copy.wait()
+    for copy in late_loads:
+        copy.start()
 
     @pl.loop(0, ROWS // 16, unroll=4)
     def _(i):
@@ -220,9 +241,9 @@
             to_slots(read, store, perm)
 
     gather_rows(0)
-    for c in loads[1:4]:
-        c.wait()
-    own = pltpu.make_async_copy(staged.at[cc], kv.at[cc, z, xc], load_sem.at[7])
+    for copy in kv_loads:
+        copy.wait()
+    own = pltpu.make_async_copy(staged.at[cc], kv.at[cc, z, xc], load_sem.at[15])
     own.start()
     pl.semaphore_wait(barrier, NEP + 1)
 
@@ -295,6 +316,10 @@
         for h in range(2):
 
             def go(zi, j, p):
+                if h == 0:
+                    remote(
+                        wsend.at[p], wrecv.at[p], w_send, w_recv.at[c], ep_dev(place_of(zi, j))
+                    ).start()
                 remote(
                     send.at[h, message(p)],
                     recv.at[h, message(p)],
@@ -302,10 +327,6 @@
                     disp_recv.at[2 * c + h],
                     ep_dev(place_of(zi, j)),
                 ).start()
-                if h == 0:
-                    remote(
-                        wsend.at[p], wrecv.at[p], w_send, w_recv.at[c], ep_dev(place_of(zi, j))
-                    ).start()
 
             for_partners(c, go)
         if c == 0:
@@ -323,6 +344,9 @@
         wsend.at[own_place], wrecv.at[own_place], w_recv.at[own_chunk]
     ).start()
 
+    for c in range(CHUNKS):
+        place[c] = jnp.where(slot - c * SLOTS == iota((ROWS, SLOTS), 1), 1.0, 0.0).astype(BF)
+
     y_copies = {}
 
     def y_copy(c, i, src, dst, t):
@@ -342,23 +366,23 @@
             xg[c, h, 0, b * 16 : (b + 1) * 16, k * 128 : (k + 1) * 128] = value
 
         from_slots(read, store, perm)
-        y_copy(c, 2 * h, xg.at[c, h, 0], xg.at[c, h, 1], right)
-        y_copy(c, 2 * h + 1, xg.at[c, h, 0], xg.at[c, h, 2], left)
-        if h == 1:
+        if h == 0:
             wait_bytes(wrecv.at[pl.ds(c * 16, 16)], w_recv.at[c])
             wgat[c, 0] = jnp.sum(wrecv[c * 16 : (c + 1) * 16].reshape(2, 8, 128), axis=1)
             y_copy(c, 4, wgat.at[c, 0], wgat.at[c, 1], right)
             y_copy(c, 5, wgat.at[c, 0], wgat.at[c, 2], left)
+        y_copy(c, 2 * h, xg.at[c, h, 0], xg.at[c, h, 1], right)
+        y_copy(c, 2 * h + 1, xg.at[c, h, 0], xg.at[c, h, 2], left)
 
     def gather_second(c, h):
         if h == 0:
             y_copies[c, 0].wait_recv()
+            y_copies[c, 4].wait_recv()
+            y_copy(c, 8, wgat.at[c, 1], wgat.at[c, 3], right)
             y_copy(c, 6, xg.at[c, 0, 1], xg.at[c, 0, 3], right)
         else:
             y_copies[c, 3].wait_recv()
             y_copy(c, 7, xg.at[c, 1, 2], xg.at[c, 1, 3], left)
-            y_copies[c, 4].wait_recv()
-            y_copy(c, 8, wgat.at[c, 1], wgat.at[c, 3], right)
 
     def experts(c):
         for i in (1, 2, 5, 6, 7, 8):
@@ -378,7 +402,7 @@
         column = jnp.sum(jnp.where(j == lane, weights, 0.0), axis=1, keepdims=True)
 
         def down(h):
-            @pl.loop(0, HALF // 512)
+            @pl.loop(0, HALF // 512, unroll=2)
             def _(n):
                 at = pl.ds(pl.multiple_of(n * 512, 512), 512)
                 wide = pl.ds(pl.multiple_of(n * 512 + h * HALF, 512), 512)
@@ -392,7 +416,7 @@
         y_copy(c, 11, part.at[c, 0, 1], fr.at[c, 0], left)
 
     def add_to(c, h, r, ref):
-        @pl.loop(0, HALF // 512)
+        @pl.loop(0, HALF // 512, unroll=2)
         def _(n):
             at = pl.ds(pl.multiple_of(n * 512, 512), 512)
             part[c, h, r, :, at] = (
@@ -413,7 +437,7 @@
         y_copies[c, 12 + h].wait_recv()
         y_copies[c, 11 + 3 * h].wait_recv()
 
-        @pl.loop(0, HALF // 512)
+        @pl.loop(0, HALF // 512, unroll=2)
         def _(n):
             at = pl.ds(pl.multiple_of(n * 512, 512), 512)
             mixed[:, at] = (
@@ -456,7 +480,7 @@
 
         from_slots(read, store, perm)
 
-        @pl.loop(0, HALF // 512)
+        @pl.loop(0, HALF // 512, unroll=2)
         def _(n):
             at = pl.ds(pl.multiple_of(n * 512, 512), 512)
             wide = pl.ds(pl.multiple_of(n * 512 + h * HALF, 512), 512)
@@ -516,50 +540,50 @@
     gather_second(0, 1)
     gather_first(1, 0)
     gather_first(1, 1)
+    gather_second(1, 0)
     gather_first(2, 0)
+    gather_second(1, 1)
+    for copy in late_loads:
+        copy.wait()
+    experts(0)
+    gather_second(2, 0)
     gather_first(2, 1)
-    for c in loads[4:7]:
-        c.wait()
-    experts(0)
-    gather_second(1, 0)
-    gather_second(1, 1)
+    reduce_second(0, 0)
+    experts(1)
+    gather_first(3, 0)
+    kv_along_x()
     gather_second(2, 1)
-    reduce_second(0, 0)
-    kv_along_x()
+    reduce_second(1, 0)
+    gather_first(3, 1)
+    reduce_second(1, 1)
     give_back(0, 0)
-    gather_first(3, 0)
-    gather_first(3, 1)
-    experts(1)
-    gather_second(2, 0)
+    give_back(1, 0)
     reduce_second(0, 1)
-    finish(0, 0)
-    reduce_second(1, 0)
-    reduce_second(1, 1)
     gather_second(3, 1)
     experts(2)
-    give_back(1, 0)
     gather_second(3, 0)
+    finish(0, 0)
+    kv_across()
     give_back(0, 1)
-    kv_across()
     give_back(1, 1)
     reduce_second(2, 0)
     wait_bytes(kv.at[0], kv_recv.at[6])
-    attend(1)
-    finish(1, 0)
+    attend(0)
     reduce_second(2, 1)
     experts(3)
     give_back(2, 0)
+    finish(1, 0)
+    finish(0, 1)
     give_back(2, 1)
-    finish(0, 1)
     reduce_second(3, 0)
+    finish(1, 1)
     reduce_second(3, 1)
+    attend(1)
     give_back(3, 0)
-    finish(1, 1)
     finish(2, 0)
     give_back(3, 1)
+    finish(3, 0)
     finish(2, 1)
-    attend(0)
-    finish(3, 0)
     finish(3, 1)
 
     for copy in y_copies.values():
@@ -595,6 +619,11 @@
     hbm = pl.BlockSpec(memory_space=pl.ANY)
     sem = pltpu.SemaphoreType.DMA
     scratch = [
+        pltpu.VMEM((ROWS, HEADS * HEAD), BF),
+        pltpu.VMEM((1, D), F32),
+        pltpu.VMEM((1, ROWS), jnp.int32),
+        pltpu.VMEM((2, ROWS), jnp.int32),
+        pltpu.VMEM((2, ROWS), F32),
         pltpu.VMEM((ROWS, D), BF),
         pltpu.VMEM((ROWS, D), BF),
         pltpu.VMEM((CHUNKS * SLOTS, D), BF),
@@ -623,7 +652,7 @@
         pltpu.VMEM((2, ROWS, HEAD), BF),
         pltpu.VMEM((2, NZ, NX * NC, ROWS, HEAD), BF),
         pltpu.VMEM((NZ, NX * NC, HEADS, ROWS), F32),
-        sem((8,)),
+        sem((16,)),
         sem,
         sem((2 * CHUNKS,)),
         sem,
@@ -642,7 +671,7 @@
             pltpu.VMEM((ROWS, HEADS * HEAD), BF),
             pltpu.VMEM((ROWS, D), BF),
         ),
-        in_specs=[vmem, hbm, hbm, hbm, hbm, vmem, vmem, vmem, vmem, hbm, hbm, hbm],
+        in_specs=[hbm] * 12,
         out_specs=(vmem, vmem),
         scratch_shapes=scratch,
         compiler_params=pltpu.CompilerParams(

time: 141 us -> 140 us (level); the launches traced: 141 us -> 138 us
  Pallas kernels: 139 us -> 136 us
    pallas_call x1, Pallas kernels: 139 us -> 136 us  [per_device(): pl.pallas_call(kernel, name='step', out_shape=(pltpu.VMEM((ROWS, HEADS *...]
where the time goes in v4:
time: 140 us; the launch traced here: 138 us
  Pallas kernels  136 us (97%)
  local copies, waits for them, and re-layouts  1.63 us (1%)
    pallas_call x1, Pallas kernels, per_device(): pl.pallas_call(kernel, name='step', out_shape=(pltpu.VMEM((ROWS, HEADS *...  136 us

profile of v4, /device:TPU:1, one launch (start us, length us, event | category | flops | bytes accessed | tf_op | source)
XLA Modules:
  0.0 138.5 jit_solution(3713126823454164590)
XLA Ops:
  0.6 136.2 %step.1 = (bf16[128,512]{1,0:T(8,128)(2,1)S(1)}, bf16[128,4096]{1,0:T(8,128)(2,1)S(1)}) custom-call(bf16[128,512]{1,0:T(8,128)(2,1)} %q_hbm.1, bf16[128,128]{1,0:T(8,128)(2,1)} %keys_ref.1, bf16[128,128]{1,0:T(8,128)(2,1)} %values_ref.1, f32[4,128]{1,0:T(4,128)} %bitcast.12, bf16[128,4096]{1,0:T(8,128)(2,1)} %x_hbm.1, f32[1,4096]{1,0:T(1,128)} %bitcast.11, ...), custom_call_target="tpu_custom_call" | custom-call | tf_op jit(solution)/shard_map/step/pallas_call | solution.py:667
  136.8 0.7 copy.16
  137.5 1.0 copy.17
